TPU v7x, 32 devices: a whole 2x2x4 slice. The times are simulated.
32 devices in a mesh: sp: 16 (over z, y, x), tp: 2 (over core).
Axes of the slice: x: 2, y: 2, z: 4, core: 2. Of those that a mesh axis runs over, the one named last changes fastest.
Arguments:
- resid: bfloat16 [6144, 2048], P('sp', 'tp'), may hold values from -40 to 40
- query_one: bfloat16 [6144, 1024], P('sp', 'tp'), may hold values from -64 to 64
- key_one: bfloat16 [6144, 1024], P('sp', 'tp'), may hold values from -64 to 64
- query_two: bfloat16 [6144, 1024], P('sp', 'tp'), may hold values from -64 to 64
- key_two: bfloat16 [6144, 1024], P('sp', 'tp'), may hold values from -64 to 64
- values: bfloat16 [6144, 2048], P('sp', 'tp'), may hold values from -6 to 6
- mix_lambda: float32 [8], P('tp'), may hold values from 0.3 to 0.8
- segments: int32 [6144], P('sp'), may hold values from 0 to 7, never falling along the last dimension, each value on 1 to 1536 neighbouring positions
- head_gain: float32 [256], replicated, may hold values from 0.1 to 1.9
- out_weight: bfloat16 [2048, 2048], P(None, 'tp'), may hold values from -0.125 to 0.125
- mixer_gain: float32 [2048], P('tp'), may hold values from 0.1 to 1.9
- gate_weight: bfloat16 [2048, 6144], P('sp', 'tp'), may hold values from -0.125 to 0.125
- up_weight: bfloat16 [2048, 6144], P('sp', 'tp'), may hold values from -0.125 to 0.125
- down_weight: bfloat16 [6144, 2048], P('tp', 'sp'), may hold values from -0.078125 to 0.078125
Outputs:
- layer_out: bfloat16 [6144, 2048], P('sp', 'tp')
Inputs may be any that keep to these rules, and one draw needn't show every extreme that they name: `segments`: numbers never fall along the sequence; each document has at most 1536 positions and one has exactly that many.
All inputs are finite; a program needn't handle non-finite values.
Results may differ from a plain program's by a relative error of at most 0.012.
Values may be sent and summed in bfloat16 or wider, within the bound.
No kernel may reach another device: no remote copies, remote signals or barrier semaphores. Data moves between devices by JAX's collectives and lax.ppermute only.
A program may use at most 128 MiB of HBM per device.

v0:
```python
import jax
import jax.numpy as jnp
from jax import lax
from jax.sharding import PartitionSpec as P

HD = 128
VD = 256
REACH = 4


def shifted(value, axis, by):
    length = lax.axis_size(axis)
    pairs = [(i, i + by) for i in range(length) if 0 <= i + by < length]
    return lax.ppermute(value, axis, pairs)


def body(
    resid,
    query_one,
    key_one,
    query_two,
    key_two,
    values,
    mix_lambda,
    segments,
    head_gain,
    out_weight,
    mixer_gain,
    gate_weight,
    up_weight,
    down_weight,
):
    rows = query_one.shape[0]
    heads = mix_lambda.shape[0]
    position = lax.axis_index("sp")
    carried = (key_one, key_two, values, segments)
    earlier = [carried]
    for step in range(REACH):
        carried = shifted((carried[0], carried[1], carried[2], carried[3]), "sp", 1)
        earlier.insert(0, carried)
    width = (REACH + 1) * rows
    k_first = jnp.concatenate([piece[0] for piece in earlier], 0).reshape(width, heads, HD)
    k_second = jnp.concatenate([piece[1] for piece in earlier], 0).reshape(width, heads, HD)
    vals = jnp.concatenate([piece[2] for piece in earlier], 0).reshape(width, heads, VD)
    seg_key = jnp.concatenate([piece[3] for piece in earlier], 0)
    q_pos = position * rows + jnp.arange(rows, dtype=jnp.int32)
    k_pos = (position - REACH) * rows + jnp.arange(width, dtype=jnp.int32)
    allowed = (
        (seg_key[None, :] == segments[:, None])
        & (k_pos[None, :] <= q_pos[:, None])
        & (k_pos[None, :] >= 0)
    )

    def weights(query, keys):
        score = jnp.einsum(
            "qhd,khd->hqk", query.reshape(rows, heads, HD), keys, preferred_element_type=jnp.float32
        ) * HD ** (-0.5)
        score = jnp.where(allowed[None], score, -jnp.inf)
        score = score - jnp.max(score, axis=-1, keepdims=True)
        expo = jnp.exp(score)
        return (expo / jnp.sum(expo, axis=-1, keepdims=True)).astype(jnp.bfloat16)

    out_first = jnp.einsum(
        "hqk,khe->qhe", weights(query_one, k_first), vals, preferred_element_type=jnp.float32
    )
    out_second = jnp.einsum(
        "hqk,khe->qhe", weights(query_two, k_second), vals, preferred_element_type=jnp.float32
    )
    head_out = out_first - mix_lambda[None, :, None] * out_second
    meansq = jnp.mean(head_out * head_out, axis=-1, keepdims=True)
    attn_rows = (
        (head_out * lax.rsqrt(meansq + 1e-05) * head_gain)
        .reshape(rows, heads * VD)
        .astype(jnp.bfloat16)
    )
    projected = jnp.dot(
        lax.all_gather(attn_rows, "tp", axis=1, tiled=True),
        out_weight,
        preferred_element_type=jnp.float32,
    )
    mid = (resid.astype(jnp.float32) + projected).astype(jnp.bfloat16)
    midf = mid.astype(jnp.float32)
    squares = lax.psum(jnp.sum(midf * midf, axis=1), "tp")
    channels = mid.shape[1] * lax.axis_size("tp")
    normed = (midf * lax.rsqrt(squares / channels + 1e-06)[:, None] * mixer_gain).astype(
        jnp.bfloat16
    )
    whole_rows = lax.all_gather(normed, "tp", axis=1, tiled=True)
    gate = jnp.dot(
        whole_rows,
        lax.all_gather(gate_weight, "sp", axis=0, tiled=True),
        preferred_element_type=jnp.float32,
    )
    up = jnp.dot(
        whole_rows,
        lax.all_gather(up_weight, "sp", axis=0, tiled=True),
        preferred_element_type=jnp.float32,
    )
    hidden = (jax.nn.silu(gate) * up).astype(jnp.bfloat16)
    terms = jnp.dot(
        hidden,
        lax.all_gather(down_weight, "sp", axis=1, tiled=True),
        preferred_element_type=jnp.float32,
    )
    summed = lax.psum_scatter(
        terms.astype(jnp.bfloat16), "tp", scatter_dimension=1, tiled=True
    ).astype(jnp.float32)
    return (midf + summed).astype(jnp.bfloat16)


def solution(mesh):
    in_specs = (
        P("sp", "tp"),
        P("sp", "tp"),
        P("sp", "tp"),
        P("sp", "tp"),
        P("sp", "tp"),
        P("sp", "tp"),
        P("tp"),
        P("sp"),
        P(),
        P(None, "tp"),
        P("tp"),
        P("sp", "tp"),
        P("sp", "tp"),
        P("tp", "sp"),
    )
    out_specs = P("sp", "tp")
    return jax.shard_map(body, mesh=mesh, in_specs=in_specs, out_specs=out_specs, check_vma=False)
```

profile of v0, /device:TPU:18, one launch (start us, length us, event | category | flops | bytes accessed | tf_op | source)
XLA Modules:
  0.0 767.5 jit_solution(17959958012359783923)
XLA Ops:
  6.5 1.3 copy.26
  7.8 3.4 collective-permute-start.12
  11.2 3.4 collective-permute-start.4
  14.6 3.4 collective-permute-start
  18.0 1.2 copy.21
  19.2 3.4 collective-permute-start.8
  22.7 3.4 collective-permute-start.5
  26.1 3.4 collective-permute-start.13
  29.5 17.5 %collective-permute-done.5 = s32[384]{0:T(512)S(1)} collective-permute-done((s32[384]{0:T(512)S(1)}, s32[384]{0:T(512)S(1)}, u32[]{:S(2)}, u32[]{:S(2)}) %collective-permute-start.5) | collective-permute-done | bytes 1568 | tf_op jit(solution)/shard_map/ppermute | solution.py:14
  47.0 4.3 collective-permute-start.6
  51.4 3.0 collective-permute-done.6
  54.4 4.3 collective-permute-start.7
  58.7 1.5 collective-permute-done.7
  60.2 4.9 collective-permute-start.9
  65.1 2.6 collective-permute-start.14
  68.4 7.4 collective-permute-done.9
  75.9 4.0 collective-permute-start.10
  79.8 4.4 collective-permute-done.14
  84.3 4.0 collective-permute-start.15
  88.3 2.5 and_and_fusion
  90.9 3.3 collective-permute-start.1
  94.2 6.2 collective-permute-start.11
  101.3 1.1 constant_dynamic-update-slice_fusion.13
  103.5 6.2 fusion.19
  109.6 17.4 %fusion.30 = (f32[4,384]{1,0:T(4,128)S(1)}, f32[4,384,1920]{1,2,0:T(8,128)}) fusion(f32[4,1920,384]{2,1,0:T(8,128)} %fusion.19, pred[384,1920]{0,1:T(8,128)(4,1)S(1)} %and_and_fusion), kind=kOutput, calls=%fused_computation.71 | output fusion | flops 17696640 | bytes 24336384 | tf_op jit(solution)/shard_map/sub | solution.py:59
  127.0 4.1 collective-permute-start.2
  132.2 1.1 constant_dynamic-update-slice_fusion.9
  133.2 1.1 constant_dynamic-update-slice_fusion.8
  134.5 6.1 fusion.22
  140.6 4.6 collective-permute-done.2
  145.1 3.9 collective-permute-start.3
  149.0 17.7 %fusion.31 = (f32[4,384]{1,0:T(4,128)S(1)}, f32[4,384,1920]{1,2,0:T(8,128)}) fusion(f32[4,1920,384]{2,1,0:T(8,128)} %fusion.22, pred[384,1920]{0,1:T(8,128)(4,1)} %copy-done.4), kind=kOutput, calls=%fused_computation.72 | output fusion | flops 17696640 | bytes 24336384 | tf_op jit(solution)/shard_map/sub | solution.py:59
  171.5 6.3 copy.20
  177.8 8.0 %fusion.9 = f32[4,256,384]{2,1,0:T(8,128)S(1)} fusion(bf16[1920,4,256]{0,2,1:T(8,128)(2,1)} %bitcast.60, f32[4,384,1920]{1,2,0:T(8,128)} %get-tuple-element.6, f32[4,384]{1,0:T(4,128)S(1)} %get-tuple-element.5), kind=kOutput, calls=%fused_computation.15 | convolution fusion | flops 1515847680 | bytes 17307648 | tf_op jit(solution)/shard_map/hqk,khe->qhe/dot_general | solution.py:66
  185.8 6.8 fusion.16
  192.6 1.1 fusion.18
  194.0 12.7 %all-gather.6.cloned.1.call-done = bf16[384,2048]{0,1:T(8,128)(2,1)} async-done(((bf16[384,1024]{0,1:T(8,128)(2,1)}), bf16[384,2048]{0,1:T(8,128)(2,1)}) %all-gather.6.cloned.1.call-update) | async-done | bytes 1572880 | tf_op jit(solution)/shard_map/all_gather | solution.py:77
  206.7 4.6 fusion.12
  211.3 2.5 psum.7
  213.7 1.1 fusion.14
  216.9 9.2 %all-gather.8.cloned.1.call-done = bf16[384,2048]{1,0:T(8,128)(2,1)} async-done(((bf16[384,1024]{1,0:T(8,128)(2,1)}), bf16[384,2048]{1,0:T(8,128)(2,1)}) %all-gather.8.cloned.1.call-update) | async-done | bytes 1572880 | tf_op jit(solution)/shard_map/all_gather | solution.py:88
  226.0 154.2 %all-gather.10.cloned.1.call-done = bf16[2048,3072]{1,0:T(8,128)(2,1)} async-done(((bf16[128,3072]{1,0:T(8,128)(2,1)}), bf16[2048,3072]{1,0:T(8,128)(2,1)}) %all-gather.10.cloned.1.call-update) | async-done | bytes 12582928 | tf_op jit(solution)/shard_map/all_gather | solution.py:91
  380.3 9.9 %fusion.32 = f32[384,3072]{1,0:T(8,128)} fusion(bf16[384,2048]{1,0:T(8,128)(2,1)} %all-gather.8.cloned.1.call-done, bf16[2048,3072]{1,0:T(8,128)(2,1)} %all-gather.10.cloned.1.call-done), kind=kOutput, calls=%fused_computation.73 | convolution fusion | flops 4831838208 | bytes 18874368 | tf_op jit(solution)/shard_map/dot_general | solution.py:89
  390.1 142.4 %all-gather.12.cloned.1.call-done = bf16[2048,3072]{1,0:T(8,128)(2,1)} async-done(((bf16[128,3072]{1,0:T(8,128)(2,1)}), bf16[2048,3072]{1,0:T(8,128)(2,1)}) %all-gather.12.cloned.1.call-update) | async-done | bytes 12582928 | tf_op jit(solution)/shard_map/all_gather | solution.py:96
  532.5 195.3 %all-gather.14.cloned.1.call-done = bf16[3072,2048]{1,0:T(8,128)(2,1)} async-done(((bf16[3072,128]{1,0:T(8,128)(2,1)}), bf16[3072,2048]{1,0:T(8,128)(2,1)}) %all-gather.14.cloned.1.call-update) | async-done | bytes 12582928 | tf_op jit(solution)/shard_map/all_gather | solution.py:102
  727.8 21.0 %convolution_convert_fusion = bf16[384,2048]{1,0:T(8,128)(2,1)} fusion(bf16[3072,2048]{1,0:T(8,128)(2,1)} %all-gather.14.cloned.1.call-done, f32[384,3072]{1,0:T(8,128)} %fusion.32, bf16[384,2048]{1,0:T(8,128)(2,1)S(1)} %copy-done.13, bf16[2048,3072]{1,0:T(8,128)(2,1)} %all-gather.12.cloned.1.call-done), kind=kOutput, calls=%fused_computation.20 | convolution fusion | flops 9671540736 | bytes 33030144 | tf_op jit(solution)/shard_map/dot_general | solution.py:100
  748.9 9.5 %reduce-scatter.2.cloned.1.call-done = bf16[384,1024]{1,0:T(8,128)(2,1)} async-done(((bf16[384,2048]{1,0:T(8,128)(2,1)}), bf16[384,1024]{1,0:T(8,128)(2,1)}) %reduce-scatter.2.cloned.1.call-update) | async-done | bytes 786448 | tf_op jit(solution)/shard_map/reduce_scatter | solution.py:105
  758.3 2.3 fusion.15
  (77 shorter events, 11.0 us)
Async XLA Ops:
  6.5 96.9 %copy-start = (bf16[384,512]{1,0:T(8,128)(2,1)S(1)}, bf16[384,512]{1,0:T(8,128)(2,1)}, u32[]{:S(2)}) copy-start(bf16[384,512]{1,0:T(8,128)(2,1)} %param.17) | copy-start | bytes 1179652
  6.5 200.1 %all-gather.6.cloned.1.call-start = ((), (), s32[]{:S(2)}) async-start(), calls=%async_computation.1 | async-start | bytes 2359296 | tf_op jit(solution)/shard_map/all_gather | solution.py:77
  7.8 18.3 %collective-permute-start.12 = (bf16[384,512]{0,1:T(8,128)(2,1)S(1)}, bf16[384,512]{0,1:T(8,128)(2,1)S(1)}, u32[]{:S(2)}, u32[]{:S(2)}) collective-permute-start(bf16[384,512]{0,1:T(8,128)(2,1)S(1)} %copy.26), channel_id=1, source_target_pairs={{0,2},{2,4},{4,6},{6,8},{8,10},{10,12},{12,14},{14,16},{16,18},{18... | collective-permute-start | bytes 1179656 | tf_op jit(solution)/shard_map/ppermute | solution.py:14
  11.2 11.4 %collective-permute-start.4 = (s32[384]{0:T(512)}, s32[384]{0:T(512)S(1)}, u32[]{:S(2)}, u32[]{:S(2)}) collective-permute-start(s32[384]{0:T(512)} %param.21), channel_id=1, source_target_pairs={{0,2},{2,4},{4,6},{6,8},{8,10},{10,12},{12,14},{14,16},{16,18},{18... | collective-permute-start | bytes 4616 | tf_op jit(solution)/shard_map/ppermute | solution.py:14
  14.6 76.2 %collective-permute-start = (bf16[384,1024]{1,0:T(8,128)(2,1)}, bf16[384,1024]{1,0:T(8,128)(2,1)S(1)}, u32[]{:S(2)}, u32[]{:S(2)}) collective-permute-start(bf16[384,1024]{1,0:T(8,128)(2,1)} %param.19), channel_id=1, source_target_pairs={{0,2},{2,4},{4,6},{6,8},{8,10},{10,12},{12,14},{14,16},{16,18},{18... | collective-permute-start | bytes 2359304 | tf_op jit(solution)/shard_map/ppermute | solution.py:14
  19.2 40.9 %collective-permute-start.8 = (bf16[384,512]{0,1:T(8,128)(2,1)S(1)}, bf16[384,512]{0,1:T(8,128)(2,1)S(1)}, u32[]{:S(2)}, u32[]{:S(2)}) collective-permute-start(bf16[384,512]{0,1:T(8,128)(2,1)S(1)} %copy.21), channel_id=1, source_target_pairs={{0,2},{2,4},{4,6},{6,8},{8,10},{10,12},{12,14},{14,16},{16,18},{18... | collective-permute-start | bytes 1179656 | tf_op jit(solution)/shard_map/ppermute | solution.py:14
  22.7 24.4 %collective-permute-start.5 = (s32[384]{0:T(512)S(1)}, s32[384]{0:T(512)S(1)}, u32[]{:S(2)}, u32[]{:S(2)}) collective-permute-start(s32[384]{0:T(512)S(1)} %collective-permute-done.4), channel_id=1, source_target_pairs={{0,2},{2,4},{4,6},{6,8},{8,10},{10,12},{12,14},{14,16},{16,18},{18... | collective-permute-start | bytes 4616 | tf_op jit(solution)/shard_map/ppermute | solution.py:14
  26.1 64.7 %copy-start.8 = (bf16[384,512]{0,1:T(8,128)(2,1)}, bf16[384,512]{0,1:T(8,128)(2,1)S(1)}, u32[]{:S(2)}) copy-start(bf16[384,512]{0,1:T(8,128)(2,1)S(1)} %collective-permute-done.12) | copy-start | bytes 1179652
  26.1 39.0 %collective-permute-start.13 = (bf16[384,512]{0,1:T(8,128)(2,1)S(1)}, bf16[384,512]{0,1:T(8,128)(2,1)S(1)}, u32[]{:S(2)}, u32[]{:S(2)}) collective-permute-start(bf16[384,512]{0,1:T(8,128)(2,1)S(1)} %collective-permute-done.12), channel_id=1, source_target_pairs={{0,2},{2,4},{4,6},{6,8},{8,10},{10,12},{12,14},{14,16},{16,18},{18... | collective-permute-start | bytes 1179656 | tf_op jit(solution)/shard_map/ppermute | solution.py:14
  47.0 7.3 collective-permute-start.6
  54.4 5.8 collective-permute-start.7
  60.2 30.7 %copy-start.6 = (bf16[384,512]{0,1:T(8,128)(2,1)}, bf16[384,512]{0,1:T(8,128)(2,1)S(1)}, u32[]{:S(2)}) copy-start(bf16[384,512]{0,1:T(8,128)(2,1)S(1)} %collective-permute-done.8) | copy-start | bytes 1179652
  60.2 15.7 %collective-permute-start.9 = (bf16[384,512]{0,1:T(8,128)(2,1)S(1)}, bf16[384,512]{0,1:T(8,128)(2,1)S(1)}, u32[]{:S(2)}, u32[]{:S(2)}) collective-permute-start(bf16[384,512]{0,1:T(8,128)(2,1)S(1)} %collective-permute-done.8), channel_id=1, source_target_pairs={{0,2},{2,4},{4,6},{6,8},{8,10},{10,12},{12,14},{14,16},{16,18},{18... | collective-permute-start | bytes 1179656 | tf_op jit(solution)/shard_map/ppermute | solution.py:14
  65.1 19.2 %copy-start.9 = (bf16[384,512]{0,1:T(8,128)(2,1)}, bf16[384,512]{0,1:T(8,128)(2,1)S(1)}, u32[]{:S(2)}) copy-start(bf16[384,512]{0,1:T(8,128)(2,1)S(1)} %collective-permute-done.13) | copy-start | bytes 1179652
  65.1 19.2 %collective-permute-start.14 = (bf16[384,512]{0,1:T(8,128)(2,1)S(1)}, bf16[384,512]{0,1:T(8,128)(2,1)S(1)}, u32[]{:S(2)}, u32[]{:S(2)}) collective-permute-start(bf16[384,512]{0,1:T(8,128)(2,1)S(1)} %collective-permute-done.13), channel_id=1, source_target_pairs={{0,2},{2,4},{4,6},{6,8},{8,10},{10,12},{12,14},{14,16},{16,18},{18... | collective-permute-start | bytes 1179656 | tf_op jit(solution)/shard_map/ppermute | solution.py:14
  75.9 27.6 %copy-start.10 = (bf16[384,512]{0,1:T(8,128)(2,1)}, bf16[384,512]{0,1:T(8,128)(2,1)S(1)}, u32[]{:S(2)}) copy-start(bf16[384,512]{0,1:T(8,128)(2,1)S(1)} %collective-permute-done.9) | copy-start | bytes 1179652
  75.9 18.3 %collective-permute-start.10 = (bf16[384,512]{0,1:T(8,128)(2,1)S(1)}, bf16[384,512]{0,1:T(8,128)(2,1)}, u32[]{:S(2)}, u32[]{:S(2)}) collective-permute-start(bf16[384,512]{0,1:T(8,128)(2,1)S(1)} %collective-permute-done.9), channel_id=1, source_target_pairs={{0,2},{2,4},{4,6},{6,8},{8,10},{10,12},{12,14},{14,16},{16,18},{18... | collective-permute-start | bytes 1179656 | tf_op jit(solution)/shard_map/ppermute | solution.py:14
  84.3 16.9 %collective-permute-start.15 = (bf16[384,512]{0,1:T(8,128)(2,1)S(1)}, bf16[384,512]{0,1:T(8,128)(2,1)S(1)}, u32[]{:S(2)}, u32[]{:S(2)}) collective-permute-start(bf16[384,512]{0,1:T(8,128)(2,1)S(1)} %collective-permute-done.14), channel_id=1, source_target_pairs={{0,2},{2,4},{4,6},{6,8},{8,10},{10,12},{12,14},{14,16},{16,18},{18... | collective-permute-start | bytes 1179656 | tf_op jit(solution)/shard_map/ppermute | solution.py:14
  90.9 18.8 %copy-start.4 = (pred[384,1920]{0,1:T(8,128)(4,1)}, pred[384,1920]{0,1:T(8,128)(4,1)S(1)}, u32[]{:S(2)}) copy-start(pred[384,1920]{0,1:T(8,128)(4,1)S(1)} %and_and_fusion) | copy-start | bytes 2211844
  90.9 36.1 %collective-permute-start.1 = (bf16[384,1024]{1,0:T(8,128)(2,1)S(1)}, bf16[384,1024]{1,0:T(8,128)(2,1)S(1)}, u32[]{:S(2)}, u32[]{:S(2)}) collective-permute-start(bf16[384,1024]{1,0:T(8,128)(2,1)S(1)} %collective-permute-done), channel_id=1, source_target_pairs={{0,2},{2,4},{4,6},{6,8},{8,10},{10,12},{12,14},{14,16},{16,18},{18... | collective-permute-start | bytes 2359304 | tf_op jit(solution)/shard_map/ppermute | solution.py:14
  94.2 36.9 %collective-permute-start.11 = (bf16[384,512]{0,1:T(8,128)(2,1)}, bf16[384,512]{0,1:T(8,128)(2,1)}, u32[]{:S(2)}, u32[]{:S(2)}) collective-permute-start(bf16[384,512]{0,1:T(8,128)(2,1)} %collective-permute-done.10), channel_id=1, source_target_pairs={{0,2},{2,4},{4,6},{6,8},{8,10},{10,12},{12,14},{14,16},{16,18},{18... | collective-permute-start | bytes 1179656 | tf_op jit(solution)/shard_map/ppermute | solution.py:14
  109.6 24.7 %copy-start.7 = (bf16[384,512]{0,1:T(8,128)(2,1)S(1)}, bf16[384,512]{0,1:T(8,128)(2,1)}, u32[]{:S(2)}) copy-start(bf16[384,512]{0,1:T(8,128)(2,1)} %copy-done.6) | copy-start | bytes 1179652
  127.0 7.5 copy-start.5
  127.0 18.1 %collective-permute-start.2 = (bf16[384,1024]{1,0:T(8,128)(2,1)S(1)}, bf16[384,1024]{1,0:T(8,128)(2,1)S(1)}, u32[]{:S(2)}, u32[]{:S(2)}) collective-permute-start(bf16[384,1024]{1,0:T(8,128)(2,1)S(1)} %collective-permute-done.1), channel_id=1, source_target_pairs={{0,2},{2,4},{4,6},{6,8},{8,10},{10,12},{12,14},{14,16},{16,18},{18... | collective-permute-start | bytes 2359304 | tf_op jit(solution)/shard_map/ppermute | solution.py:14
  145.1 21.6 %collective-permute-start.3 = (bf16[384,1024]{1,0:T(8,128)(2,1)S(1)}, bf16[384,1024]{1,0:T(8,128)(2,1)S(1)}, u32[]{:S(2)}, u32[]{:S(2)}) collective-permute-start(bf16[384,1024]{1,0:T(8,128)(2,1)S(1)} %collective-permute-done.2), channel_id=1, source_target_pairs={{0,2},{2,4},{4,6},{6,8},{8,10},{10,12},{12,14},{14,16},{16,18},{18... | collective-permute-start | bytes 2359304 | tf_op jit(solution)/shard_map/ppermute | solution.py:14
  166.7 3.8 copy-start.3
  177.8 8.0 %copy-start.2 = (bf16[1920,1024]{0,1:T(8,128)(2,1)S(1)}, bf16[1920,1024]{0,1:T(8,128)(2,1)}, u32[]{:S(2)}) copy-start(bf16[1920,1024]{0,1:T(8,128)(2,1)} %copy.20) | copy-start | bytes 11796484
  177.8 8.0 %copy-start.15 = (f32[4]{0:T(128)S(1)}, f32[4]{0:T(128)}, u32[]{:S(2)}) copy-start(f32[4]{0:T(128)} %param.20) | copy-start | bytes 52
  185.8 6.8 copy-start.12
  185.8 20.9 %copy-start.14 = (bf16[384,1024]{1,0:T(8,128)(2,1)S(1)}, bf16[384,1024]{1,0:T(8,128)(2,1)}, u32[]{:S(2)}) copy-start(bf16[384,1024]{1,0:T(8,128)(2,1)} %param.14) | copy-start | bytes 2359300
  193.7 20.0 %copy-start.11 = (f32[1024]{0:T(1024)S(1)}, f32[1024]{0:T(1024)}, u32[]{:S(2)}) copy-start(f32[1024]{0:T(1024)} %param.24) | copy-start | bytes 12292
  193.7 32.3 %all-gather.8.cloned.1.call-start = ((), (), s32[]{:S(2)}) async-start(), calls=%async_computation.2 | async-start | bytes 2359296 | tf_op jit(solution)/shard_map/all_gather | solution.py:88
  214.9 165.3 %all-gather.10.cloned.1.call-start = ((), (), s32[]{:S(2)}) async-start(), calls=%async_computation.3 | async-start | bytes 13369344 | tf_op jit(solution)/shard_map/all_gather | solution.py:91
  215.6 316.9 %all-gather.12.cloned.1.call-start = ((), (), s32[]{:S(2)}) async-start(), calls=%async_computation.4 | async-start | bytes 13369344 | tf_op jit(solution)/shard_map/all_gather | solution.py:96
  216.2 511.6 %all-gather.14.cloned.1.call-start = ((), (), s32[]{:S(2)}) async-start(), calls=%async_computation.5 | async-start | bytes 13369344 | tf_op jit(solution)/shard_map/all_gather | solution.py:102
  216.8 541.5 %reduce-scatter.2.cloned.1.call-start = ((), (), s32[]{:S(2)}) async-start(), calls=%async_computation.6 | async-start | bytes 2359296 | tf_op jit(solution)/shard_map/reduce_scatter | solution.py:105
  226.0 501.8 %copy-start.13 = (bf16[384,2048]{1,0:T(8,128)(2,1)S(1)}, bf16[384,2048]{1,0:T(8,128)(2,1)}, u32[]{:S(2)}) copy-start(bf16[384,2048]{1,0:T(8,128)(2,1)} %all-gather.8.cloned.1.call-done) | copy-start | bytes 4718596
  727.8 32.8 %copy-start.1 = (bf16[384,512]{1,0:T(8,128)(2,1)S(1)}, bf16[384,512]{1,0:T(8,128)(2,1)}, u32[]{:S(2)}) copy-start(bf16[384,512]{1,0:T(8,128)(2,1)} %param.17) | copy-start | bytes 1179652
Sparse Core Ops, SparseCore 0:
  193.8 12.7 all-gather.5
  215.0 10.9 all-gather.7
  228.8 151.3 all-gather.9
  382.9 149.5 all-gather.11
  535.1 192.7 all-gather.13
  749.0 9.3 reduce-scatter.1
where the time goes:
time: 770 us; the launch traced here: 767 us
  waiting for transfers between devices  564 us (73%)
  matrix products  62.5 us (8%)
  starting transfers between devices  62.3 us (8%)
  other arithmetic  42.2 us (5%)
  local copies, waits for them, and re-layouts  19.9 us (3%)
  between operations  13.9 us (2%)
    all_gather x1, waiting for transfers between devices, body(): lax.all_gather(down_weight, 'sp', axis=1, tiled=True)  195 us
    all_gather x1, waiting for transfers between devices, body(): lax.all_gather(gate_weight, 'sp', axis=0, tiled=True)  154 us
    all_gather x1, waiting for transfers between devices, body(): lax.all_gather(up_weight, 'sp', axis=0, tiled=True)  142 us
    ppermute x16, starting transfers between devices, shifted(): return lax.ppermute(value, axis, pairs)  61.9 us
    ppermute x16, waiting for transfers between devices, shifted(): return lax.ppermute(value, axis, pairs)  39.2 us
    sub x2, other arithmetic, weights(): score = score - jnp.max(score, axis=-1, keepdims=True)  35.1 us
    dot_general x1, matrix products, body(): jnp.dot(hidden, lax.all_gather(down_weight, 'sp', axis=1, tiled=True), pr...  21 us
  transfers between devices with their start and end apart: 22, of which 13 were waited for; matrix products, arithmetic and copies ran while one was open for 9% of the time, Pallas kernels for 0%

commit v1 on v0

v1 whole, which is shorter than its diff:
```python
import math

import jax
import jax.numpy as jnp
from jax import lax
from jax.experimental import pallas as pl
from jax.experimental.pallas import tpu as pltpu
from jax.sharding import Mesh, PartitionSpec as P

HD = 128
VD = 256
REACH = 4
QB = 128


def swap(value):
    return lax.ppermute(value, "tp", [(0, 1), (1, 0)])


def tp_gather(value, axis):
    if lax.axis_size("tp") != 2:
        return lax.all_gather(value, "tp", axis=axis, tiled=True)
    other = swap(value)
    first = lax.axis_index("tp") == 0
    return jnp.concatenate(
        [jnp.where(first, value, other), jnp.where(first, other, value)], axis
    )


def tp_sum(value):
    if lax.axis_size("tp") != 2:
        return lax.psum(value, "tp")
    return value + swap(value)


def tp_reduce_scatter(value):
    if lax.axis_size("tp") != 2:
        return lax.psum_scatter(value, "tp", scatter_dimension=1, tiled=True).astype(jnp.float32)
    half = value.shape[1] // 2
    me = lax.axis_index("tp")
    mine = lax.dynamic_slice_in_dim(value, me * half, half, 1)
    theirs = lax.dynamic_slice_in_dim(value, (1 - me) * half, half, 1)
    return mine.astype(jnp.float32) + swap(theirs).astype(jnp.float32)


def shift(value, axis, by):
    length = lax.axis_size(axis)
    return lax.ppermute(value, axis, [(i, (i + by) % length) for i in range(length)])


def attention_kernel(lam_ref, q_ref, kv_prev_ref, kv_ref, seg_q_ref, seg_k_ref, gain_ref, out_ref, kv_all):
    step = pl.program_id(1)
    rows = kv_ref.shape[1]
    span = kv_prev_ref.shape[1]

    @pl.when(step == 0)
    def _():
        kv_all[:span] = kv_prev_ref[0]
        kv_all[span:] = kv_ref[0]

    width = span + QB
    start = pl.multiple_of(step * QB, QB)
    seg_q = seg_q_ref[...]
    seg_k = seg_k_ref[:, pl.ds(start, width)]
    q_pos = lax.broadcasted_iota(jnp.int32, (QB, 1), 0) + span
    k_pos = lax.broadcasted_iota(jnp.int32, (1, width), 1)
    allowed = (seg_k == seg_q) & (k_pos <= q_pos)
    vals = kv_all[pl.ds(start, width), 2 * HD :]

    def one(which):
        query = q_ref[0, :, which * HD : (which + 1) * HD]
        keys = kv_all[pl.ds(start, width), which * HD : (which + 1) * HD]
        score = lax.dot_general(
            query, keys, (((1,), (1,)), ((), ())), preferred_element_type=jnp.float32
        )
        score = jnp.where(allowed, score * HD ** (-0.5), -1e30)
        score = score - jnp.max(score, axis=-1, keepdims=True)
        expo = jnp.exp(score)
        total = jnp.sum(expo, axis=-1, keepdims=True)
        probs = (expo * (1.0 / total)).astype(jnp.bfloat16)
        return jnp.dot(probs, vals, preferred_element_type=jnp.float32)

    head_out = one(0) - lam_ref[pl.program_id(0)] * one(1)
    meansq = jnp.mean(head_out * head_out, axis=-1, keepdims=True)
    out_ref[0] = (head_out * lax.rsqrt(meansq + 1e-05) * gain_ref[...]).astype(jnp.bfloat16)


def attention(query, kv_prev, kv, lam, seg_q, seg_k, gain):
    heads, rows, _ = query.shape
    span = kv_prev.shape[1]
    wide = 2 * HD + VD
    return pl.pallas_call(
        attention_kernel,
        grid=(heads, rows // QB),
        in_specs=[
            pl.BlockSpec(memory_space=pltpu.SMEM),
            pl.BlockSpec((1, QB, 2 * HD), lambda h, i: (h, i, 0)),
            pl.BlockSpec((1, span, wide), lambda h, i: (h, 0, 0)),
            pl.BlockSpec((1, rows, wide), lambda h, i: (h, 0, 0)),
            pl.BlockSpec((QB, 1), lambda h, i: (i, 0)),
            pl.BlockSpec((1, span + rows), lambda h, i: (0, 0)),
            pl.BlockSpec((1, VD), lambda h, i: (0, 0)),
        ],
        out_specs=pl.BlockSpec((1, QB, VD), lambda h, i: (h, i, 0)),
        out_shape=jax.ShapeDtypeStruct((heads, rows, VD), jnp.bfloat16),
        scratch_shapes=[pltpu.VMEM((span + rows, wide), jnp.bfloat16)],
        compiler_params=pltpu.CompilerParams(
            dimension_semantics=("arbitrary", "arbitrary"), vmem_limit_bytes=48 * 2**20
        ),
        cost_estimate=pl.CostEstimate(
            flops=heads * rows * (span + QB) * (2 * HD + 2 * VD) * 2,
            bytes_accessed=heads * (span + 3 * rows) * wide * 2,
            transcendentals=heads * rows * (span + QB) * 2,
        ),
        name="diff_attention",
    )(lam, query, kv_prev, kv, seg_q, seg_k, gain)


def body(
    resid,
    query_one,
    key_one,
    query_two,
    key_two,
    values,
    mix_lambda,
    segments,
    head_gain,
    out_weight,
    mixer_gain,
    gate_weight,
    up_weight,
    down_weight,
):
    rows = query_one.shape[0]
    heads = mix_lambda.shape[0]
    group = lax.axis_size("sg")
    planes = lax.axis_size("sz")
    plane = lax.axis_index("sz")
    member = lax.axis_index("sg")
    hidden = gate_weight.shape[1] // group
    krows = gate_weight.shape[0]
    dcols = down_weight.shape[1]

    gate_up = jnp.concatenate(
        [gate_weight.reshape(krows, group, hidden), up_weight.reshape(krows, group, hidden)], 2
    ).transpose(1, 0, 2)
    gate_up = lax.all_to_all(gate_up, "sg", 0, 0, tiled=True).reshape(group * krows, 2 * hidden)

    kv = jnp.concatenate(
        [
            key_one.reshape(rows, heads, HD),
            key_two.reshape(rows, heads, HD),
            values.reshape(rows, heads, VD),
        ],
        2,
    ).transpose(1, 0, 2)
    query = jnp.concatenate(
        [query_one.reshape(rows, heads, HD), query_two.reshape(rows, heads, HD)], 2
    ).transpose(1, 0, 2)
    gate_up, kv = lax.optimization_barrier((gate_up, kv))
    gate_up = lax.all_gather(gate_up, "sz", axis=0, tiled=True)
    seg_all = lax.all_gather(segments, ("sz", "sg"), axis=0, tiled=True)
    gain = head_gain.reshape(1, VD)
    ahead = [(i, i + 1) for i in range(planes - 1)]

    split = heads % group == 0 and group >= REACH
    if split:
        each = heads // group
        span = REACH * rows
        whole = group * rows

        def to_heads(x):
            x = lax.all_to_all(x.reshape(group, each, rows, -1), "sg", 0, 0, tiled=True)
            return x.transpose(1, 0, 2, 3).reshape(each, whole, -1)

        kv = to_heads(kv)
        kv_prev = lax.ppermute(kv[:, whole - span :], "sz", ahead)
        kv_barred, query = lax.optimization_barrier((kv, query))
        query = to_heads(query)
        lam = lax.dynamic_slice_in_dim(mix_lambda, member * each, each, 0)
        first = plane * whole
    else:
        span = REACH * rows
        whole = rows
        count = group * planes
        lam = mix_lambda
        pieces = [
            lax.ppermute(kv, ("sz", "sg"), [(i, i + by) for i in range(count - by)])
            for by in range(REACH, 0, -1)
        ]
        kv_prev = jnp.concatenate(pieces, 1)
        first = (plane * group + member) * rows

    seg_pad = jnp.concatenate([jnp.full((span,), -1, jnp.int32), seg_all.astype(jnp.int32)])
    seg_k = lax.dynamic_slice_in_dim(seg_pad, first, span + whole, 0)
    seg_q = seg_k[span:].reshape(whole, 1)
    attn = attention(query, kv_prev, kv, lam, seg_q, seg_k.reshape(1, span + whole), gain)

    down = down_weight.reshape(group, hidden, dcols)
    down, query_done = lax.optimization_barrier((down, query))
    down = lax.all_to_all(down, "sg", 0, 0, tiled=True)
    down = lax.all_gather(down, "sz", axis=0, tiled=True)

    if split:
        back = attn.reshape(each, group, rows, VD).transpose(1, 0, 2, 3)
        back = lax.all_to_all(back, "sg", 0, 0, tiled=True).reshape(heads, rows, VD)
    else:
        back = attn
    attn_rows = back.transpose(1, 0, 2).reshape(rows, heads * VD)
    projected = jnp.dot(tp_gather(attn_rows, 1), out_weight, preferred_element_type=jnp.float32)
    mid = (resid.astype(jnp.float32) + projected).astype(jnp.bfloat16)
    midf = mid.astype(jnp.float32)
    squares = tp_sum(jnp.sum(midf * midf, axis=1))
    channels = mid.shape[1] * lax.axis_size("tp")
    normed = (midf * lax.rsqrt(squares / channels + 1e-06)[:, None] * mixer_gain).astype(
        jnp.bfloat16
    )

    blocks = [normed] + [shift(normed, "sg", by) for by in range(1, group)]
    whole_rows = tp_gather(jnp.concatenate(blocks, 0), 1)
    both = jnp.dot(whole_rows, gate_up, preferred_element_type=jnp.float32)
    act = (jax.nn.silu(both[:, :hidden]) * both[:, hidden:]).astype(jnp.bfloat16)
    down_full = down.transpose(1, 0, 2).reshape(hidden, planes * group * dcols)
    terms = jnp.dot(act, down_full, preferred_element_type=jnp.float32).astype(jnp.bfloat16)
    part = tp_reduce_scatter(terms)
    total = part[:rows]
    send = part.astype(jnp.bfloat16)
    for by in range(1, group):
        total = total + shift(send[by * rows : (by + 1) * rows], "sg", -by).astype(jnp.float32)
    return (midf + total).astype(jnp.bfloat16)


def solution(mesh):
    count, cores = mesh.shape["sp"], mesh.shape["tp"]
    group = math.gcd(count, REACH)
    grid = Mesh(mesh.devices.reshape(count // group, group, cores), ("sz", "sg", "tp"))
    sp = ("sz", "sg")
    in_specs = (
        P(sp, "tp"),
        P(sp, "tp"),
        P(sp, "tp"),
        P(sp, "tp"),
        P(sp, "tp"),
        P(sp, "tp"),
        P("tp"),
        P(sp),
        P(),
        P(None, "tp"),
        P("tp"),
        P(sp, "tp"),
        P(sp, "tp"),
        P("tp", sp),
    )
    return jax.shard_map(
        body, mesh=grid, in_specs=in_specs, out_specs=P(sp, "tp"), check_vma=False
    )
```

time: 770 us -> 372 us (0.48)
  waiting for transfers between devices: 564 us -> 113 us
  blocking collectives: 2.47 us -> 147 us
  starting transfers between devices: 62.3 us -> 18.3 us
  matrix products: 62.5 us -> 23.7 us
  other arithmetic: 42.2 us -> 16.2 us
  Pallas kernels: 0 us -> 19.7 us
    all_gather x5 -> x2, waiting for transfers between devices: 514 us -> 0.01 us  [the longest x1 0.01 us: body(): down = lax.all_gather(down, 'sz', axis=0, tiled=True)]
    all_gather x0 -> x1, blocking collectives: none -> 110 us  [body(): seg_all = lax.all_gather(segments, ('sz', 'sg'), axis=0, tiled=True)]
    ppermute x16 -> x11, starting transfers between devices: 61.9 us -> 9.62 us  [the longest x6 5.81 us: shift(): lax.ppermute(value, axis, [(i, (i + by) % length) for i in range(length)])]
    ppermute x16 -> x11, waiting for transfers between devices: 39.2 us -> 80.2 us  [the longest x6 69.8 us: shift(): lax.ppermute(value, axis, [(i, (i + by) % length) for i in range(length)])]
    dot_general x7 -> x3, matrix products: 62.5 us -> 23.7 us  [the longest x1 14 us: body(): both = jnp.dot(whole_rows, gate_up, preferred_element_type=jnp.float32)]
    all_to_all x0 -> x3, blocking collectives: none -> 37 us  [the longest x1 13.6 us: body(): down = lax.all_to_all(down, 'sg', 0, 0, tiled=True)]
    sub x2 -> x0, other arithmetic: 35.1 us -> none  [weights(): score = score - jnp.max(score, axis=-1, keepdims=True)]
    all_to_all x0 -> x2, waiting for transfers between devices: none -> 32.7 us  [the longest x1 17.6 us: to_heads(): x = lax.all_to_all(x.reshape(group, each, rows, -1), 'sg', 0, 0, tiled=True)]
  transfers between devices with their start and end apart: 22 -> 15, of which waited for: 13 -> 11; matrix products, arithmetic and copies ran while one was open for 9% -> 6% of each run, Pallas kernels for 0% -> 5%
where the time goes in v1:
time: 372 us
  blocking collectives  147 us (40%)
  waiting for transfers between devices  113 us (30%)
  matrix products  23.7 us (6%)
  local copies, waits for them, and re-layouts  20.2 us (5%)
  Pallas kernels  19.7 us (5%)
  starting transfers between devices  18.3 us (5%)
  other arithmetic  16.2 us (4%)
  between operations  13.7 us (4%)
    all_gather x1, blocking collectives, body(): seg_all = lax.all_gather(segments, ('sz', 'sg'), axis=0, tiled=True)  110 us
    ppermute x6, waiting for transfers between devices, shift(): lax.ppermute(value, axis, [(i, (i + by) % length) for i in range(length)])  69.8 us
    pallas_call x1, Pallas kernels, attention(): pl.pallas_call(attention_kernel, grid=(heads, rows // QB), in_specs=[pl.B...  19.7 us
    all_to_all x1, waiting for transfers between devices, to_heads(): x = lax.all_to_all(x.reshape(group, each, rows, -1), 'sg', 0, 0, tiled=True)  17.6 us
    all_to_all x1, waiting for transfers between devices, body(): lax.all_to_all(gate_up, 'sg', 0, 0, tiled=True)  15 us
    dot_general x1, matrix products, body(): both = jnp.dot(whole_rows, gate_up, preferred_element_type=jnp.float32)  14 us
    all_to_all x1, blocking collectives, body(): down = lax.all_to_all(down, 'sg', 0, 0, tiled=True)  13.6 us
    all_to_all x1, blocking collectives, to_heads(): x = lax.all_to_all(x.reshape(group, each, rows, -1), 'sg', 0, 0, tiled=True)  12.9 us
  transfers between devices with their start and end apart: 15, of which 11 were waited for; matrix products, arithmetic and copies ran while one was open for 6% of the time, Pallas kernels for 5%

profile of v1, /device:TPU:18, one launch (start us, length us, event | category | flops | bytes accessed | tf_op | source)
XLA Modules:
  0.0 371.6 jit_solution(3830921931352371829)
XLA Ops:
  6.5 1.5 copy.44
  8.0 1.5 copy.45
  9.6 1.3 maximum_bitcast_fusion
  10.9 4.4 %all-to-all-start = ((bf16[4,128,1536]{1,2,0:T(8,128)(2,1)}), bf16[4,128,1536]{1,2,0:T(8,128)(2,1)S(1)}, u32[]{:S(2)}, u32[]{:S(2)}) async-start(bf16[4,128,1536]{1,2,0:T(8,128)(2,1)} %maximum_bitcast_fusion), calls=%async_computation | async-start | bytes 3145728 | tf_op jit(solution)/shard_map/all_to_all | solution.py:148
  15.3 1.2 copy.49
  16.6 0.9 copy.48
  17.6 1.4 maximum_bitcast_fusion.1
  19.0 15.0 %all-to-all-done = bf16[4,128,1536]{1,2,0:T(8,128)(2,1)S(1)} async-done(((bf16[4,128,1536]{1,2,0:T(8,128)(2,1)}), bf16[4,128,1536]{1,2,0:T(8,128)(2,1)S(1)}, u32[]{:S(2)}, u32[]{:S(2)}) %all-to-all-start) | async-done | bytes 1572896 | tf_op jit(solution)/shard_map/all_to_all | solution.py:148
  34.0 1.6 copy.46
  35.6 1.7 copy.50
  37.3 4.3 %all-to-all-start.1 = ((bf16[4,1,384,512]{3,2,1,0:T(8,128)(2,1)}), bf16[4,1,384,512]{3,2,1,0:T(8,128)(2,1)S(1)}, u32[]{:S(2)}, u32[]{:S(2)}) async-start(bf16[4,1,384,512]{3,2,1,0:T(8,128)(2,1)} %copy.50), calls=%async_computation.1 | async-start | bytes 3145728 | tf_op jit(solution)/shard_map/all_to_all | solution.py:174
  42.1 17.6 %all-to-all-done.1 = bf16[4,1,384,512]{3,2,1,0:T(8,128)(2,1)S(1)} async-done(((bf16[4,1,384,512]{3,2,1,0:T(8,128)(2,1)}), bf16[4,1,384,512]{3,2,1,0:T(8,128)(2,1)S(1)}, u32[]{:S(2)}, u32[]{:S(2)}) %all-to-all-start.1) | async-done | bytes 1572896 | tf_op jit(solution)/shard_map/all_to_all | solution.py:174
  59.7 0.3 copy.53
  60.0 12.9 %all_to_all.25 = bf16[4,1,384,256]{3,2,1,0:T(8,128)(2,1)S(1)} all-to-all(bf16[4,1,384,256]{3,2,1,0:T(8,128)(2,1)S(1)} %copy.53), channel_id=1, replica_groups=mesh['sz'=4,'sg'=4,'tp'=2] {'sg'}, dimensions={0} | all-to-all | bytes 1572864 | tf_op jit(solution)/shard_map/all_to_all | solution.py:174
  72.9 13.6 %all_to_all.26 = bf16[4,768,128]{2,1,0:T(8,128)(2,1)} all-to-all(bf16[4,768,128]{2,1,0:T(8,128)(2,1)} %bitcast.54), channel_id=1, replica_groups=mesh['sz'=4,'sg'=4,'tp'=2] {'sg'}, dimensions={0} | all-to-all | bytes 1572864 | tf_op jit(solution)/shard_map/all_to_all | solution.py:202
  86.6 3.5 collective-permute-start
  90.1 110.0 %all-gather = s32[16,1,384]{2,1,0:T(1,128)S(1)} all-gather(s32[1,1,384]{2,1,0:T(1,128)S(1)} %reshape.70), channel_id=1, replica_groups=mesh['sz'=4,'sg'=4,'tp'=2] {'sz','sg'}, dimensions={0}, use_global_device_ids=true | all-gather | bytes 26112 | tf_op jit(solution)/shard_map/all_gather | solution.py:163
  200.2 0.3 reshape.72.seg_q_ref
  200.4 0.6 dynamic_slice.12.lam_ref
  201.1 19.7 %diff_attention.1 = bf16[1,1536,256]{2,1,0:T(8,128)(2,1)S(1)} custom-call(f32[1]{0:T(128)} %dynamic_slice.12.lam_ref, bf16[1,1536,256]{2,1,0:T(8,128)(2,1)S(1)} %bitcast.38, bf16[1,1536,512]{2,1,0:T(8,128)(2,1)} %collective-permute-done.kv_prev_ref, bf16[1,1536,512]{2,1,0:T(8,128)(2,1)S(1)} %bitcast.37, s32[1536,1]{1,0:T(8,128)S(1)} %reshape.72.seg_q_ref, ...), custom_call_target="tpu_custom_call" | custom-call | flops 3925868544 | bytes 6291456 | tf_op jit(solution)/shard_map/diff_attention/pallas_call | solution.py:92
  220.8 0.9 copy-done
  221.7 1.6 copy.55
  223.2 10.5 %all_to_all.27 = bf16[4,1,384,256]{2,3,1,0:T(8,128)(2,1)S(1)} all-to-all(bf16[4,1,384,256]{2,3,1,0:T(8,128)(2,1)S(1)} %copy.55), channel_id=1, replica_groups=mesh['sz'=4,'sg'=4,'tp'=2] {'sg'}, dimensions={0} | all-to-all | bytes 1572864 | tf_op jit(solution)/shard_map/all_to_all | solution.py:207
  233.8 2.3 collective-permute-done.1
  236.3 4.2 %fusion.7 = (f32[384]{0:T(512)S(1)}, bf16[384,1024]{1,0:T(8,128)(2,1)S(1)}) fusion(bf16[2048,1024]{1,0:T(8,128)(2,1)} %param.23, bf16[384,1024]{0,1:T(8,128)(2,1)S(1)} %get-tuple-element.21, bf16[384,1024]{0,1:T(8,128)(2,1)S(1)} %get-tuple-element.20, bf16[384,1024]{1,0:T(8,128)(2,1)S(1)} %copy-done.13), kind=kOutput, calls=%fused_computation.15 | convolution fusion | flops 1616117376 | bytes 7341568 | tf_op jit(solution)/shard_map/dot_general | solution.py:211
  240.7 1.0 collective-permute-done.2
  241.8 0.2 fusion.9
  242.0 1.5 collective-permute-start.3
  243.5 1.1 collective-permute-start.4
  244.6 17.8 %collective-permute-done.3 = bf16[384,1024]{1,0:T(8,128)(2,1)S(1)} collective-permute-done((bf16[384,1024]{1,0:T(8,128)(2,1)S(1)}, bf16[384,1024]{1,0:T(8,128)(2,1)S(1)}, u32[]{:S(2)}, u32[]{:S(2)}) %collective-permute-start.3) | collective-permute-done | bytes 786464 | tf_op jit(solution)/shard_map/ppermute | solution.py:48
  262.5 17.2 %collective-permute-done.4 = bf16[384,1024]{1,0:T(8,128)(2,1)S(1)} collective-permute-done((bf16[384,1024]{1,0:T(8,128)(2,1)S(1)}, bf16[384,1024]{1,0:T(8,128)(2,1)S(1)}, u32[]{:S(2)}, u32[]{:S(2)}) %collective-permute-start.4) | collective-permute-done | bytes 786464 | tf_op jit(solution)/shard_map/ppermute | solution.py:48
  279.7 1.9 pad_maximum_fusion
  281.7 4.6 %copy.56 = bf16[16,768,128]{1,2,0:T(8,128)(2,1)} copy(bf16[16,768,128]{2,1,0:T(8,128)(2,1)} %all-gather.6.cloned.1.call-done) | data formatting | bytes 6291456 | tf_op jit(solution)/shard_map/all_gather | solution.py:203
  286.3 1.4 collective-permute-done.6
  287.7 4.8 %broadcast_select_fusion.1 = (bf16[1536,1024]{1,0:T(8,128)(2,1)}, bf16[1536,1024]{1,0:T(8,128)(2,1)}) fusion(bf16[1536,1024]{1,0:T(8,128)(2,1)} %collective-permute-done.6, pred[]{:T(512)S(6)} %eq.4, bf16[384,1024]{1,0:T(8,128)(2,1)S(1)} %collective-permute-done.5, bf16[384,1024]{1,0:T(8,128)(2,1)S(1)} %collective-permute-done.4, ...), kind=kLoop, calls=%fused_computation.10 | loop fusion | flops 15728640 | bytes 12582913 | tf_op jit(solution)/shard_map/jit(_where)/select_n | solution.py:26
  292.5 14.0 %fusion = f32[1536,1536]{1,0:T(8,128)S(1)} fusion(bf16[2048,1536]{1,0:T(8,128)(2,1)} %all-gather.4.cloned.1.call-done, bf16[1536,1024]{1,0:T(8,128)(2,1)} %get-tuple-element.16, bf16[1536,1024]{1,0:T(8,128)(2,1)} %get-tuple-element.15), kind=kOutput, calls=%fused_computation.1 | convolution fusion | flops 9676259328 | bytes 22020096 | tf_op jit(solution)/shard_map/dot_general | solution.py:222
  306.5 5.5 %convolution_convert_fusion = bf16[1536,2048]{1,0:T(8,128)(2,1)S(1)} fusion(bf16[768,2048]{0,1:T(8,128)(2,1)S(1)} %bitcast.44, f32[1536,1536]{1,0:T(8,128)S(1)} %fusion), kind=kOutput, calls=%fused_computation | convolution fusion | flops 4842061824 | bytes 18874368 | tf_op jit(solution)/shard_map/dot_general | solution.py:225
  312.0 0.5 constant_dynamic-slice_fusion
  312.5 2.2 copy-done.2
  314.8 5.7 %collective-permute-done.7 = bf16[1536,1024]{1,0:T(8,128)(2,1)} collective-permute-done((bf16[1536,1024]{1,0:T(8,128)(2,1)S(1)}, bf16[1536,1024]{1,0:T(8,128)(2,1)}, u32[]{:S(2)}, u32[]{:S(2)}) %collective-permute-start.7) | collective-permute-done | bytes 3145760 | tf_op jit(solution)/shard_map/ppermute | solution.py:17
  320.4 4.5 %fusion.22 = (bf16[1536,1024]{1,0:T(8,128)(2,1)S(1)}, f32[1536,1024]{1,0:T(8,128)S(1)}) fusion(bf16[1536,1024]{1,0:T(8,128)(2,1)} %collective-permute-done.7, bf16[1536,2048]{1,0:T(8,128)(2,1)} %copy-done.2, s32[]{:T(128)S(6)} %select_n.44), kind=kLoop, calls=%fused_computation.39 | loop fusion | flops 6291456 | bytes 15728644 | tf_op jit(solution)/shard_map/convert_element_type | solution.py:228
  325.2 0.9 collective-permute-start.10
  326.1 1.2 collective-permute-start.8
  327.3 1.1 collective-permute-start.9
  328.4 17.3 %collective-permute-done.10 = bf16[384,1024]{1,0:T(8,128)(2,1)S(1)} collective-permute-done((bf16[384,1024]{1,0:T(8,128)(2,1)S(1)}, bf16[384,1024]{1,0:T(8,128)(2,1)S(1)}, u32[]{:S(2)}, u32[]{:S(2)}) %collective-permute-start.10) | collective-permute-done | bytes 786464 | tf_op jit(solution)/shard_map/ppermute | solution.py:48
  345.6 16.7 %collective-permute-done.8 = bf16[384,1024]{1,0:T(8,128)(2,1)S(1)} collective-permute-done((bf16[384,1024]{1,0:T(8,128)(2,1)S(1)}, bf16[384,1024]{1,0:T(8,128)(2,1)S(1)}, u32[]{:S(2)}, u32[]{:S(2)}) %collective-permute-start.8) | collective-permute-done | bytes 786464 | tf_op jit(solution)/shard_map/ppermute | solution.py:48
  362.3 0.8 collective-permute-done.9
  363.1 1.6 fusion.10
  (51 shorter events, 1.8 us)
Async XLA Ops:
  9.6 5.7 %copy-start.6 = (bf16[384,1024]{1,0:T(8,128)(2,1)S(1)}, bf16[384,1024]{1,0:T(8,128)(2,1)}, u32[]{:S(2)}) copy-start(bf16[384,1024]{1,0:T(8,128)(2,1)} %param.19) | copy-start | bytes 2359300
  10.9 5.5 %copy-start.7 = (bf16[384,512]{1,0:T(8,128)(2,1)S(1)}, bf16[384,512]{1,0:T(8,128)(2,1)}, u32[]{:S(2)}) copy-start(bf16[384,512]{1,0:T(8,128)(2,1)} %param.16) | copy-start | bytes 1179652
  10.9 5.8 %copy-start.8 = (bf16[384,512]{1,0:T(8,128)(2,1)S(1)}, bf16[384,512]{1,0:T(8,128)(2,1)}, u32[]{:S(2)}) copy-start(bf16[384,512]{1,0:T(8,128)(2,1)} %param.18) | copy-start | bytes 1179652
  10.9 23.1 %all-to-all-start = ((bf16[4,128,1536]{1,2,0:T(8,128)(2,1)}), bf16[4,128,1536]{1,2,0:T(8,128)(2,1)S(1)}, u32[]{:S(2)}, u32[]{:S(2)}) async-start(bf16[4,128,1536]{1,2,0:T(8,128)(2,1)} %maximum_bitcast_fusion), calls=%async_computation | async-start | bytes 3145728 | tf_op jit(solution)/shard_map/all_to_all | solution.py:148
  35.6 5.9 %copy-start.9 = (bf16[384,512]{1,0:T(8,128)(2,1)S(1)}, bf16[384,512]{1,0:T(8,128)(2,1)}, u32[]{:S(2)}) copy-start(bf16[384,512]{1,0:T(8,128)(2,1)} %param.15) | copy-start | bytes 1179652
  37.3 4.5 %copy-start.10 = (bf16[384,512]{1,0:T(8,128)(2,1)S(1)}, bf16[384,512]{1,0:T(8,128)(2,1)}, u32[]{:S(2)}) copy-start(bf16[384,512]{1,0:T(8,128)(2,1)} %param.17) | copy-start | bytes 1179652
  37.3 22.4 %all-to-all-start.1 = ((bf16[4,1,384,512]{3,2,1,0:T(8,128)(2,1)}), bf16[4,1,384,512]{3,2,1,0:T(8,128)(2,1)S(1)}, u32[]{:S(2)}, u32[]{:S(2)}) async-start(bf16[4,1,384,512]{3,2,1,0:T(8,128)(2,1)} %copy.50), calls=%async_computation.1 | async-start | bytes 3145728 | tf_op jit(solution)/shard_map/all_to_all | solution.py:174
  41.5 240.1 %all-gather.6.cloned.1.call-start = ((), (), s32[]{:S(2)}) async-start(), calls=%async_computation.6 | async-start | bytes 3932160 | tf_op jit(solution)/shard_map/all_gather | solution.py:203
  60.0 30.1 %copy-start.12 = (s32[384]{0:T(512)S(1)}, s32[384]{0:T(512)}, u32[]{:S(2)}) copy-start(s32[384]{0:T(512)} %param.21) | copy-start | bytes 4612
  60.0 140.5 %copy-start.14 = (f32[4]{0:T(128)S(1)}, f32[4]{0:T(128)}, u32[]{:S(2)}) copy-start(f32[4]{0:T(128)} %param.20) | copy-start | bytes 52
  60.0 141.1 %copy-start.1 = (f32[256]{0:T(256)S(1)}, f32[256]{0:T(256)}, u32[]{:S(2)}) copy-start(f32[256]{0:T(256)} %param.22) | copy-start | bytes 3076
  86.5 206.0 %all-gather.4.cloned.1.call-start = ((), (), s32[]{:S(2)}) async-start(), calls=%async_computation.5 | async-start | bytes 7864320 | tf_op jit(solution)/shard_map/all_gather | solution.py:162
  86.6 114.5 %collective-permute-start = (bf16[1,1536,512]{2,1,0:T(8,128)(2,1)S(1)}, bf16[1,1536,512]{2,1,0:T(8,128)(2,1)}, u32[]{:S(2)}, u32[]{:S(2)}) collective-permute-start(bf16[1,1536,512]{2,1,0:T(8,128)(2,1)S(1)} %bitcast.36), channel_id=1, source_target_pairs={{0,8},{8,16},{16,24},{1,9},{9,17},{17,25},{2,10},{10,18},{18,26},{... | collective-permute-start | bytes 4718600 | tf_op jit(solution)/shard_map/ppermute | solution.py:178
  220.8 0.9 copy-start
  221.7 14.6 %copy-start.13 = (bf16[384,1024]{1,0:T(8,128)(2,1)S(1)}, bf16[384,1024]{1,0:T(8,128)(2,1)}, u32[]{:S(2)}) copy-start(bf16[384,1024]{1,0:T(8,128)(2,1)} %param.14) | copy-start | bytes 2359300
  233.8 2.3 collective-permute-start.1
  236.3 5.5 %copy-start.11 = (f32[1024]{0:T(1024)S(1)}, f32[1024]{0:T(1024)}, u32[]{:S(2)}) copy-start(f32[1024]{0:T(1024)} %param.24) | copy-start | bytes 12292
  240.5 39.2 %copy-start.4 = (bf16[384,1024]{1,0:T(8,128)(2,1)}, bf16[384,1024]{1,0:T(8,128)(2,1)S(1)}, u32[]{:S(2)}) copy-start(bf16[384,1024]{1,0:T(8,128)(2,1)S(1)} %get-tuple-element.23) | copy-start | bytes 2359300
  240.5 1.2 collective-permute-start.2
  242.0 20.5 %collective-permute-start.3 = (bf16[384,1024]{1,0:T(8,128)(2,1)S(1)}, bf16[384,1024]{1,0:T(8,128)(2,1)S(1)}, u32[]{:S(2)}, u32[]{:S(2)}) collective-permute-start(bf16[384,1024]{1,0:T(8,128)(2,1)S(1)} %fusion.9), channel_id=1, source_target_pairs={{0,2},{2,4},{4,6},{6,0},{1,3},{3,5},{5,7},{7,1},{8,10},{10,12},{12... | collective-permute-start | bytes 2359304 | tf_op jit(solution)/shard_map/ppermute | solution.py:48
  243.5 36.2 %collective-permute-start.4 = (bf16[384,1024]{1,0:T(8,128)(2,1)S(1)}, bf16[384,1024]{1,0:T(8,128)(2,1)S(1)}, u32[]{:S(2)}, u32[]{:S(2)}) collective-permute-start(bf16[384,1024]{1,0:T(8,128)(2,1)S(1)} %fusion.9), channel_id=1, source_target_pairs={{0,4},{2,6},{4,0},{6,2},{1,5},{3,7},{5,1},{7,3},{8,12},{10,14},{12... | collective-permute-start | bytes 2359304 | tf_op jit(solution)/shard_map/ppermute | solution.py:48
  244.6 35.1 %collective-permute-start.5 = (bf16[384,1024]{1,0:T(8,128)(2,1)S(1)}, bf16[384,1024]{1,0:T(8,128)(2,1)S(1)}, u32[]{:S(2)}, u32[]{:S(2)}) collective-permute-start(bf16[384,1024]{1,0:T(8,128)(2,1)S(1)} %fusion.9), channel_id=1, source_target_pairs={{0,6},{2,0},{4,2},{6,4},{1,7},{3,1},{5,3},{7,5},{8,14},{10,8},{12,... | collective-permute-start | bytes 2359304 | tf_op jit(solution)/shard_map/ppermute | solution.py:48
  281.7 6.0 %collective-permute-start.6 = (bf16[1536,1024]{1,0:T(8,128)(2,1)}, bf16[1536,1024]{1,0:T(8,128)(2,1)}, u32[]{:S(2)}, u32[]{:S(2)}) collective-permute-start(bf16[1536,1024]{1,0:T(8,128)(2,1)} %pad_maximum_fusion), channel_id=1, source_target_pairs={{0,1},{1,0},{2,3},{3,2},{4,5},{5,4},{6,7},{7,6},{8,9},{9,8},{10,11... | collective-permute-start | bytes 9437192 | tf_op jit(solution)/shard_map/ppermute | solution.py:17
  292.5 14.0 %copy-start.3 = (bf16[16,768,128]{1,2,0:T(8,128)(2,1)S(1)}, bf16[16,768,128]{1,2,0:T(8,128)(2,1)}, u32[]{:S(2)}) copy-start(bf16[16,768,128]{1,2,0:T(8,128)(2,1)} %copy.56) | copy-start | bytes 9437188
  312.0 2.6 copy-start.2
  314.6 5.8 %collective-permute-start.7 = (bf16[1536,1024]{1,0:T(8,128)(2,1)S(1)}, bf16[1536,1024]{1,0:T(8,128)(2,1)}, u32[]{:S(2)}, u32[]{:S(2)}) collective-permute-start(bf16[1536,1024]{1,0:T(8,128)(2,1)S(1)} %constant_dynamic-slice_fusion), channel_id=1, source_target_pairs={{0,1},{1,0},{2,3},{3,2},{4,5},{5,4},{6,7},{7,6},{8,9},{9,8},{10,11... | collective-permute-start | bytes 9437192 | tf_op jit(solution)/shard_map/ppermute | solution.py:17
  325.0 38.2 %copy-start.5 = (bf16[384,1024]{1,0:T(8,128)(2,1)S(1)}, bf16[384,1024]{1,0:T(8,128)(2,1)}, u32[]{:S(2)}) copy-start(bf16[384,1024]{1,0:T(8,128)(2,1)} %copy-done.4) | copy-start | bytes 2359300
  325.2 20.5 %collective-permute-start.10 = (bf16[384,1024]{1,0:T(8,128)(2,1)S(1)}, bf16[384,1024]{1,0:T(8,128)(2,1)S(1)}, u32[]{:S(2)}, u32[]{:S(2)}) collective-permute-start(bf16[384,1024]{1,0:T(8,128)(2,1)S(1)} %get-tuple-element.18), channel_id=1, source_target_pairs={{0,2},{2,4},{4,6},{6,0},{1,3},{3,5},{5,7},{7,1},{8,10},{10,12},{12... | collective-permute-start | bytes 2359304 | tf_op jit(solution)/shard_map/ppermute | solution.py:48
  326.1 36.2 %collective-permute-start.8 = (bf16[384,1024]{1,0:T(8,128)(2,1)S(1)}, bf16[384,1024]{1,0:T(8,128)(2,1)S(1)}, u32[]{:S(2)}, u32[]{:S(2)}) collective-permute-start(bf16[384,1024]{1,0:T(8,128)(2,1)S(1)} %get-tuple-element.17), channel_id=1, source_target_pairs={{0,6},{2,0},{4,2},{6,4},{1,7},{3,1},{5,3},{7,5},{8,14},{10,8},{12,... | collective-permute-start | bytes 2359304 | tf_op jit(solution)/shard_map/ppermute | solution.py:48
  327.3 35.9 %collective-permute-start.9 = (bf16[384,1024]{1,0:T(8,128)(2,1)S(1)}, bf16[384,1024]{1,0:T(8,128)(2,1)S(1)}, u32[]{:S(2)}, u32[]{:S(2)}) collective-permute-start(bf16[384,1024]{1,0:T(8,128)(2,1)S(1)} %get-tuple-element.19), channel_id=1, source_target_pairs={{0,4},{2,6},{4,0},{6,2},{1,5},{3,7},{5,1},{7,3},{8,12},{10,14},{12... | collective-permute-start | bytes 2359304 | tf_op jit(solution)/shard_map/ppermute | solution.py:48
Sparse Core Ops, SparseCore 0:
  86.7 83.5 all-gather.5
  171.8 114.3 all-gather.3

commit v2 on v1

--- a/solution.py
+++ b/solution.py
@@ -17,14 +17,35 @@
     return lax.ppermute(value, "tp", [(0, 1), (1, 0)])
 
 
-def tp_gather(value, axis):
+def halves(weight, axis):
     if lax.axis_size("tp") != 2:
-        return lax.all_gather(value, "tp", axis=axis, tiled=True)
+        return (weight, None)
+    half = weight.shape[axis] // 2
+    me = lax.axis_index("tp")
+    return (
+        lax.dynamic_slice_in_dim(weight, me * half, half, axis),
+        lax.dynamic_slice_in_dim(weight, (1 - me) * half, half, axis),
+    )
+
+
+def tp_dot(value, parts):
+    if parts[1] is None:
+        value = lax.all_gather(value, "tp", axis=1, tiled=True)
+        return jnp.dot(value, parts[0], preferred_element_type=jnp.float32)
     other = swap(value)
-    first = lax.axis_index("tp") == 0
-    return jnp.concatenate(
-        [jnp.where(first, value, other), jnp.where(first, other, value)], axis
-    )
+    return jnp.dot(value, parts[0], preferred_element_type=jnp.float32) + jnp.dot(
+        other, parts[1], preferred_element_type=jnp.float32
+    )
+
+
+def dot_scatter(value, parts):
+    if parts[1] is None:
+        terms = jnp.dot(value, parts[0], preferred_element_type=jnp.float32).astype(jnp.bfloat16)
+        terms = lax.psum_scatter(terms, "tp", scatter_dimension=1, tiled=True)
+        return terms.astype(jnp.float32)
+    away = jnp.dot(value, parts[1], preferred_element_type=jnp.float32).astype(jnp.bfloat16)
+    came = swap(away).astype(jnp.float32)
+    return jnp.dot(value, parts[0], preferred_element_type=jnp.float32) + came
 
 
 def tp_sum(value):
@@ -33,24 +54,14 @@
     return value + swap(value)
 
 
-def tp_reduce_scatter(value):
-    if lax.axis_size("tp") != 2:
-        return lax.psum_scatter(value, "tp", scatter_dimension=1, tiled=True).astype(jnp.float32)
-    half = value.shape[1] // 2
-    me = lax.axis_index("tp")
-    mine = lax.dynamic_slice_in_dim(value, me * half, half, 1)
-    theirs = lax.dynamic_slice_in_dim(value, (1 - me) * half, half, 1)
-    return mine.astype(jnp.float32) + swap(theirs).astype(jnp.float32)
-
-
-def shift(value, axis, by):
-    length = lax.axis_size(axis)
-    return lax.ppermute(value, axis, [(i, (i + by) % length) for i in range(length)])
+def mirrored(value, by):
+    if by == 0:
+        return value
+    return lax.ppermute(value, "sg", [(i, i ^ by) for i in range(lax.axis_size("sg"))])
 
 
 def attention_kernel(lam_ref, q_ref, kv_prev_ref, kv_ref, seg_q_ref, seg_k_ref, gain_ref, out_ref, kv_all):
     step = pl.program_id(1)
-    rows = kv_ref.shape[1]
     span = kv_prev_ref.shape[1]
 
     @pl.when(step == 0)
@@ -135,13 +146,16 @@
     rows = query_one.shape[0]
     heads = mix_lambda.shape[0]
     group = lax.axis_size("sg")
-    planes = lax.axis_size("sz")
-    plane = lax.axis_index("sz")
     member = lax.axis_index("sg")
     hidden = gate_weight.shape[1] // group
     krows = gate_weight.shape[0]
     dcols = down_weight.shape[1]
 
+    planes = lax.axis_size("sz")
+    ahead = [(i, i + 1) for i in range(planes - 1)]
+    seg_here = lax.all_gather(segments.astype(jnp.int32) + 1, "sg", axis=0, tiled=True)
+    seg_here, gate_weight = lax.optimization_barrier((seg_here, gate_weight))
+    seg_back = lax.ppermute(seg_here, "sz", ahead)
     gate_up = jnp.concatenate(
         [gate_weight.reshape(krows, group, hidden), up_weight.reshape(krows, group, hidden)], 2
     ).transpose(1, 0, 2)
@@ -160,9 +174,7 @@
     ).transpose(1, 0, 2)
     gate_up, kv = lax.optimization_barrier((gate_up, kv))
     gate_up = lax.all_gather(gate_up, "sz", axis=0, tiled=True)
-    seg_all = lax.all_gather(segments, ("sz", "sg"), axis=0, tiled=True)
     gain = head_gain.reshape(1, VD)
-    ahead = [(i, i + 1) for i in range(planes - 1)]
 
     split = heads % group == 0 and group >= REACH
     if split:
@@ -176,10 +188,10 @@
 
         kv = to_heads(kv)
         kv_prev = lax.ppermute(kv[:, whole - span :], "sz", ahead)
-        kv_barred, query = lax.optimization_barrier((kv, query))
+        kv, query = lax.optimization_barrier((kv, query))
         query = to_heads(query)
         lam = lax.dynamic_slice_in_dim(mix_lambda, member * each, each, 0)
-        first = plane * whole
+        first = group * rows - span
     else:
         span = REACH * rows
         whole = rows
@@ -190,16 +202,16 @@
             for by in range(REACH, 0, -1)
         ]
         kv_prev = jnp.concatenate(pieces, 1)
-        first = (plane * group + member) * rows
-
-    seg_pad = jnp.concatenate([jnp.full((span,), -1, jnp.int32), seg_all.astype(jnp.int32)])
-    seg_k = lax.dynamic_slice_in_dim(seg_pad, first, span + whole, 0)
+        first = (group + member) * rows - span
+
+    seg_both = jnp.concatenate([seg_back, seg_here])
+    seg_k = lax.dynamic_slice_in_dim(seg_both, first, span + whole, 0)
     seg_q = seg_k[span:].reshape(whole, 1)
     attn = attention(query, kv_prev, kv, lam, seg_q, seg_k.reshape(1, span + whole), gain)
 
-    down = down_weight.reshape(group, hidden, dcols)
-    down, query_done = lax.optimization_barrier((down, query))
-    down = lax.all_to_all(down, "sg", 0, 0, tiled=True)
+    down = down_weight.T.reshape(dcols, group, hidden).transpose(1, 0, 2)
+    down, _ = lax.optimization_barrier((down, query))
+    down = lax.all_to_all(down, "sg", 0, 0, tiled=True).reshape(group * dcols, hidden)
     down = lax.all_gather(down, "sz", axis=0, tiled=True)
 
     if split:
@@ -208,7 +220,7 @@
     else:
         back = attn
     attn_rows = back.transpose(1, 0, 2).reshape(rows, heads * VD)
-    projected = jnp.dot(tp_gather(attn_rows, 1), out_weight, preferred_element_type=jnp.float32)
+    projected = tp_dot(attn_rows, halves(out_weight, 0))
     mid = (resid.astype(jnp.float32) + projected).astype(jnp.bfloat16)
     midf = mid.astype(jnp.float32)
     squares = tp_sum(jnp.sum(midf * midf, axis=1))
@@ -217,17 +229,23 @@
         jnp.bfloat16
     )
 
-    blocks = [normed] + [shift(normed, "sg", by) for by in range(1, group)]
-    whole_rows = tp_gather(jnp.concatenate(blocks, 0), 1)
-    both = jnp.dot(whole_rows, gate_up, preferred_element_type=jnp.float32)
-    act = (jax.nn.silu(both[:, :hidden]) * both[:, hidden:]).astype(jnp.bfloat16)
-    down_full = down.transpose(1, 0, 2).reshape(hidden, planes * group * dcols)
-    terms = jnp.dot(act, down_full, preferred_element_type=jnp.float32).astype(jnp.bfloat16)
-    part = tp_reduce_scatter(terms)
-    total = part[:rows]
-    send = part.astype(jnp.bfloat16)
-    for by in range(1, group):
-        total = total + shift(send[by * rows : (by + 1) * rows], "sg", -by).astype(jnp.float32)
+    blocks = [mirrored(normed, by) for by in range(group)]
+    gate_up_parts = halves(gate_up, 0)
+    down_parts = [None if part is None else part.T for part in halves(down, 0)]
+    total = jnp.zeros(normed.shape, jnp.float32)
+    for first_by, last_by in [(0, 1), (1, 3), (3, 4)]:
+        chosen = list(range(first_by, min(last_by, group)))
+        if not chosen:
+            continue
+        together = jnp.concatenate([blocks[by] for by in chosen], 0)
+        both = tp_dot(together, gate_up_parts)
+        act = (jax.nn.silu(both[:, :hidden]) * both[:, hidden:]).astype(jnp.bfloat16)
+        part = dot_scatter(act, down_parts)
+        for spot, by in enumerate(chosen):
+            piece = part[spot * rows : (spot + 1) * rows]
+            if by:
+                piece = mirrored(piece.astype(jnp.bfloat16), by).astype(jnp.float32)
+            total = total + piece
     return (midf + total).astype(jnp.bfloat16)
 
 
@@ -252,6 +270,5 @@
         P(sp, "tp"),
         P("tp", sp),
     )
-    return jax.shard_map(
-        body, mesh=grid, in_specs=in_specs, out_specs=P(sp, "tp"), check_vma=False
-    )
+
+    return jax.shard_map(body, mesh=grid, in_specs=in_specs, out_specs=P(sp, "tp"), check_vma=False)

time: 372 us -> 329 us (0.88); the launches traced: 372 us -> 324 us
  blocking collectives: 147 us -> 52.7 us
  waiting for transfers between devices: 113 us -> 160 us
  other arithmetic: 16.2 us -> 6.5 us
  matrix products: 23.7 us -> 29.6 us
  starting transfers between devices: 18.3 us -> 23.9 us
    all_gather x1, blocking collectives: 110 us -> 8.1 us  [body(): lax.all_gather(segments.astype(jnp.int32) + 1, 'sg', axis=0, tiled=True)]
    ppermute x6 -> x7, waiting for transfers between devices: 69.8 us -> 146 us  [the longest x1 81.4 us: body(): seg_back = lax.ppermute(seg_here, 'sz', ahead)]
    all_to_all x1 -> x2, blocking collectives: 12.9 us -> 33.1 us  [to_heads(): x = lax.all_to_all(x.reshape(group, each, rows, -1), 'sg', 0, 0, tiled=True)]
    all_to_all x1, waiting for transfers between devices: 17.6 us -> 0.01 us  [body(): lax.all_to_all(down, 'sg', 0, 0, tiled=True).reshape(group * dcols, hidden)]
    all_to_all x1 -> x0, blocking collectives: 13.6 us -> none  [body(): down = lax.all_to_all(down, 'sg', 0, 0, tiled=True)]
    ppermute x4 -> x8, waiting for transfers between devices: 10.4 us -> 0.84 us  [swap(): return lax.ppermute(value, 'tp', [(0, 1), (1, 0)])]
    dot_general x3 -> x14, matrix products: 23.7 us -> 29.6 us  [the longest x4 11.8 us: tp_dot(): jnp.dot(value, parts[0], preferred_element_type=jnp.float32)]
    select_n x2 -> x0, other arithmetic: 5.07 us -> none  [tp_gather(): jnp.where(first, value, other)]
  transfers between devices with their start and end apart: 15 -> 20, of which waited for: 11 -> 9; matrix products, arithmetic and copies ran while one was open for 6% -> 14% of each run, Pallas kernels for 5% -> 6%
where the time goes in v2:
time: 329 us; the launch traced here: 324 us
  waiting for transfers between devices  160 us (49%)
  blocking collectives  52.7 us (16%)
  matrix products  29.6 us (9%)
  starting transfers between devices  23.9 us (7%)
  Pallas kernels  19.6 us (6%)
  local copies, waits for them, and re-layouts  17.7 us (5%)
  between operations  13.8 us (4%)
  other arithmetic  6.5 us (2%)
    ppermute x1, waiting for transfers between devices, body(): seg_back = lax.ppermute(seg_here, 'sz', ahead)  81.4 us
    ppermute x6, waiting for transfers between devices, mirrored(): lax.ppermute(value, 'sg', [(i, i ^ by) for i in range(lax.axis_size('sg'))])  64.9 us
    all_to_all x2, blocking collectives, to_heads(): x = lax.all_to_all(x.reshape(group, each, rows, -1), 'sg', 0, 0, tiled=True)  33.1 us
    pallas_call x1, Pallas kernels, attention(): pl.pallas_call(attention_kernel, grid=(heads, rows // QB), in_specs=[pl.B...  19.6 us
    all_to_all x1, waiting for transfers between devices, body(): lax.all_to_all(gate_up, 'sg', 0, 0, tiled=True)  13.2 us
    dot_general x4, matrix products, tp_dot(): jnp.dot(value, parts[0], preferred_element_type=jnp.float32)  11.8 us
    all_to_all x1, blocking collectives, body(): back = lax.all_to_all(back, 'sg', 0, 0, tiled=True).reshape(heads, rows, VD)  11.4 us
    dot_general x4, matrix products, tp_dot(): jnp.dot(other, parts[1], preferred_element_type=jnp.float32)  10.2 us
  transfers between devices with their start and end apart: 20, of which 9 were waited for; matrix products, arithmetic and copies ran while one was open for 14% of the time, Pallas kernels for 6%

profile of v2, /device:TPU:18, one launch (start us, length us, event | category | flops | bytes accessed | tf_op | source)
XLA Modules:
  0.0 324.2 jit_solution(15035269164815752794)
XLA Ops:
  6.5 1.6 copy.45
  8.2 8.1 %all-gather = s32[4,1,384]{2,1,0:T(1,128)S(1)} all-gather(s32[1,1,384]{2,1,0:T(1,128)S(1)} %reshape.70), channel_id=1, replica_groups=mesh['sz'=4,'sg'=4,'tp'=2] {'sg'}, dimensions={0}, use_global_device_ids=true | all-gather | bytes 7680 | tf_op jit(solution)/shard_map/all_gather | solution.py:156
  16.7 1.3 maximum_bitcast_fusion
  18.0 4.2 %all-to-all-start = ((bf16[4,128,1536]{1,2,0:T(8,128)(2,1)}), bf16[4,128,1536]{1,2,0:T(8,128)(2,1)S(1)}, u32[]{:S(2)}, u32[]{:S(2)}) async-start(bf16[4,128,1536]{1,2,0:T(8,128)(2,1)} %maximum_bitcast_fusion), calls=%async_computation | async-start | bytes 3145728 | tf_op jit(solution)/shard_map/all_to_all | solution.py:162
  22.2 1.2 copy.49
  23.6 0.9 copy.47
  24.5 1.4 maximum_bitcast_fusion.1
  25.9 13.2 %all-to-all-done = bf16[4,128,1536]{1,2,0:T(8,128)(2,1)S(1)} async-done(((bf16[4,128,1536]{1,2,0:T(8,128)(2,1)}), bf16[4,128,1536]{1,2,0:T(8,128)(2,1)S(1)}, u32[]{:S(2)}, u32[]{:S(2)}) %all-to-all-start) | async-done | bytes 1572896 | tf_op jit(solution)/shard_map/all_to_all | solution.py:162
  39.1 1.6 copy.46
  41.5 21.3 %all_to_all.25 = bf16[4,1,384,512]{3,2,1,0:T(8,128)(2,1)S(1)} all-to-all(bf16[4,1,384,512]{3,2,1,0:T(8,128)(2,1)S(1)} %copy.50), channel_id=1, replica_groups=mesh['sz'=4,'sg'=4,'tp'=2] {'sg'}, dimensions={0} | all-to-all | bytes 3145728 | tf_op jit(solution)/shard_map/all_to_all | solution.py:186
  62.8 3.5 %collective-permute-start = (bf16[1,1536,512]{2,1,0:T(8,128)(2,1)S(1)}, bf16[1,1536,512]{2,1,0:T(8,128)(2,1)}, u32[]{:S(2)}, u32[]{:S(2)}) collective-permute-start(bf16[1,1536,512]{2,1,0:T(8,128)(2,1)S(1)} %bitcast.46), channel_id=1, source_target_pairs={{0,8},{8,16},{16,24},{1,9},{9,17},{17,25},{2,10},{10,18},{18,26},{... | collective-permute-start | bytes 4718600 | tf_op jit(solution)/shard_map/ppermute | solution.py:190
  66.5 1.2 copy.51
  68.1 11.8 %all_to_all.26 = bf16[4,1,384,256]{3,2,1,0:T(8,128)(2,1)S(1)} all-to-all(bf16[4,1,384,256]{3,2,1,0:T(8,128)(2,1)S(1)} %copy.53), channel_id=1, replica_groups=mesh['sz'=4,'sg'=4,'tp'=2] {'sg'}, dimensions={0} | all-to-all | bytes 1572864 | tf_op jit(solution)/shard_map/all_to_all | solution.py:186
  79.9 5.4 %all-to-all-start.4 = ((bf16[4,128,768]{1,2,0:T(8,128)(2,1)}), bf16[4,128,768]{1,2,0:T(8,128)(2,1)}, u32[]{:S(2)}, u32[]{:S(2)}) async-start(bf16[4,128,768]{1,2,0:T(8,128)(2,1)} %bitcast.63), calls=%async_computation.4 | async-start | bytes 1572864 | tf_op jit(solution)/shard_map/all_to_all | solution.py:214
  85.3 1.9 collective-permute-start.1
  88.1 81.4 %collective-permute-done.1 = s32[1536]{0:T(1024)S(1)} collective-permute-done((s32[1536]{0:T(1024)S(1)}, s32[1536]{0:T(1024)S(1)}, u32[]{:S(2)}, u32[]{:S(2)}) %collective-permute-start.1) | collective-permute-done | bytes 6176 | tf_op jit(solution)/shard_map/ppermute | solution.py:158
  169.5 2.3 copy.56
  171.8 19.6 %diff_attention.1 = bf16[1,1536,256]{2,1,0:T(8,128)(2,1)S(1)} custom-call(f32[1]{0:T(128)} %dynamic_slice.21.lam_ref, bf16[1,1536,256]{2,1,0:T(8,128)(2,1)S(1)} %bitcast.48, bf16[1,1536,512]{2,1,0:T(8,128)(2,1)} %collective-permute-done.kv_prev_ref, bf16[1,1536,512]{2,1,0:T(8,128)(2,1)S(1)} %bitcast.47, s32[1536,1]{1,0:T(8,128)S(1)} %reshape.72.seg_q_ref, ...), custom_call_target="tpu_custom_call" | custom-call | flops 3925868544 | bytes 6291456 | tf_op jit(solution)/shard_map/diff_attention/pallas_call | solution.py:103
  191.5 0.9 copy-done
  192.3 1.5 copy.55
  193.8 11.4 %all_to_all.27 = bf16[4,1,384,256]{2,3,1,0:T(8,128)(2,1)S(1)} all-to-all(bf16[4,1,384,256]{2,3,1,0:T(8,128)(2,1)S(1)} %copy.55), channel_id=1, replica_groups=mesh['sz'=4,'sg'=4,'tp'=2] {'sg'}, dimensions={0} | all-to-all | bytes 1572864 | tf_op jit(solution)/shard_map/all_to_all | solution.py:219
  205.3 2.8 fusion.12
  208.4 1.2 fusion.14
  210.1 0.8 collective-permute-done.3
  211.2 1.5 collective-permute-start.12
  213.1 1.6 collective-permute-start.7
  214.7 18.0 %collective-permute-done.12 = bf16[384,1024]{1,0:T(8,128)(2,1)} collective-permute-done((bf16[384,1024]{1,0:T(8,128)(2,1)S(1)}, bf16[384,1024]{1,0:T(8,128)(2,1)}, u32[]{:S(2)}, u32[]{:S(2)}) %collective-permute-start.12) | collective-permute-done | bytes 786464 | tf_op jit(solution)/shard_map/ppermute | solution.py:60
  232.7 15.0 %collective-permute-done.6 = bf16[384,1024]{1,0:T(8,128)(2,1)S(1)} collective-permute-done((bf16[384,1024]{1,0:T(8,128)(2,1)S(1)}, bf16[384,1024]{1,0:T(8,128)(2,1)S(1)}, u32[]{:S(2)}, u32[]{:S(2)}) %collective-permute-start.6) | collective-permute-done | bytes 786464 | tf_op jit(solution)/shard_map/ppermute | solution.py:60
  247.8 1.0 constant_dynamic-update-slice_fusion.1
  248.8 0.9 constant_dynamic-update-slice_fusion
  250.3 3.7 %fusion.4 = f32[384,1536]{1,0:T(8,128)S(1)} fusion(bf16[384,1024]{1,0:T(8,128)(2,1)} %collective-permute-done.12, bf16[2048,1536]{1,0:T(8,128)(2,1)} %all-gather.4.cloned.1.call-done, s32[]{:T(128)S(6)} %select_n.14), kind=kOutput, calls=%fused_computation.8 | convolution fusion | flops 1207959552 | bytes 6291460 | tf_op jit(solution)/shard_map/dot_general | solution.py:36
  254.2 2.5 convolution_add_fusion.1
  257.1 2.4 convolution_convert_fusion.1
  259.6 5.1 %fusion.1 = f32[768,1536]{1,0:T(8,128)S(1)} fusion(bf16[768,1024]{1,0:T(8,128)(2,1)} %collective-permute-done.8, bf16[2048,1536]{1,0:T(8,128)(2,1)} %all-gather.4.cloned.1.call-done, s32[]{:T(128)S(6)} %select_n.15), kind=kOutput, calls=%fused_computation.5 | convolution fusion | flops 2415919104 | bytes 9437188 | tf_op jit(solution)/shard_map/dot_general | solution.py:36
  264.7 4.0 %convolution_add_fusion = f32[768,1536]{1,0:T(8,128)S(1)} fusion(f32[768,1536]{1,0:T(8,128)S(1)} %fusion.1, bf16[768,1024]{1,0:T(8,128)(2,1)} %constant_dynamic-update-slice_fusion, bf16[2048,1536]{1,0:T(8,128)(2,1)S(1)} %bitcast.67, s32[]{:T(128)S(6)} %select_n.14), kind=kOutput, calls=%fused_computation | convolution fusion | flops 2417098752 | bytes 14155780 | tf_op jit(solution)/shard_map/dot_general | solution.py:36
  269.4 1.2 copy-done.12
  270.6 1.4 convolution_convert_fusion
  272.5 1.4 fusion.7
  273.9 1.4 convolution_add_fusion.2
  275.9 0.8 convolution_convert_fusion.2
  276.9 0.8 add_convert_fusion.1
  277.7 2.2 collective-permute-start.15
  279.9 1.4 add_convert_fusion
  281.4 1.0 collective-permute-start.11
  282.9 0.8 fusion.27
  283.7 15.4 %collective-permute-done.15 = bf16[384,1024]{1,0:T(8,128)(2,1)S(1)} collective-permute-done((bf16[384,1024]{1,0:T(8,128)(2,1)S(1)}, bf16[384,1024]{1,0:T(8,128)(2,1)S(1)}, u32[]{:S(2)}, u32[]{:S(2)}) %collective-permute-start.15) | collective-permute-done | bytes 786464 | tf_op jit(solution)/shard_map/ppermute | solution.py:60
  299.1 16.2 %collective-permute-done.11 = bf16[384,1024]{1,0:T(8,128)(2,1)S(1)} collective-permute-done((bf16[384,1024]{1,0:T(8,128)(2,1)S(1)}, bf16[384,1024]{1,0:T(8,128)(2,1)S(1)}, u32[]{:S(2)}, u32[]{:S(2)}) %collective-permute-start.11) | collective-permute-done | bytes 786464 | tf_op jit(solution)/shard_map/ppermute | solution.py:60
  315.5 1.8 fusion.17
  (77 shorter events, 8.4 us)
Async XLA Ops:
  6.5 1.6 copy-start.10
  6.5 9.8 %copy-start.3 = (bf16[128,3072]{1,0:T(8,128)(2,1)S(1)}, bf16[128,3072]{1,0:T(8,128)(2,1)}, u32[]{:S(2)}) copy-start(bf16[128,3072]{1,0:T(8,128)(2,1)} %param.25) | copy-start | bytes 2359300
  18.0 4.2 %copy-start.4 = (bf16[384,1024]{1,0:T(8,128)(2,1)S(1)}, bf16[384,1024]{1,0:T(8,128)(2,1)}, u32[]{:S(2)}) copy-start(bf16[384,1024]{1,0:T(8,128)(2,1)} %param.19) | copy-start | bytes 2359300
  18.0 5.4 %copy-start.6 = (bf16[384,512]{1,0:T(8,128)(2,1)S(1)}, bf16[384,512]{1,0:T(8,128)(2,1)}, u32[]{:S(2)}) copy-start(bf16[384,512]{1,0:T(8,128)(2,1)} %param.18) | copy-start | bytes 1179652
  18.0 21.1 %all-to-all-start = ((bf16[4,128,1536]{1,2,0:T(8,128)(2,1)}), bf16[4,128,1536]{1,2,0:T(8,128)(2,1)S(1)}, u32[]{:S(2)}, u32[]{:S(2)}) async-start(bf16[4,128,1536]{1,2,0:T(8,128)(2,1)} %maximum_bitcast_fusion), calls=%async_computation | async-start | bytes 3145728 | tf_op jit(solution)/shard_map/all_to_all | solution.py:162
  22.2 1.4 copy-start.7
  22.2 228.1 %all-gather.4.cloned.1.call-start = ((), (), s32[]{:S(2)}) async-start(), calls=%async_computation.5 | async-start | bytes 7864320 | tf_op jit(solution)/shard_map/all_gather | solution.py:176
  41.5 24.8 %copy-start.8 = (bf16[384,512]{1,0:T(8,128)(2,1)S(1)}, bf16[384,512]{1,0:T(8,128)(2,1)}, u32[]{:S(2)}) copy-start(bf16[384,512]{1,0:T(8,128)(2,1)} %param.17) | copy-start | bytes 1179652
  62.8 109.0 %collective-permute-start = (bf16[1,1536,512]{2,1,0:T(8,128)(2,1)S(1)}, bf16[1,1536,512]{2,1,0:T(8,128)(2,1)}, u32[]{:S(2)}, u32[]{:S(2)}) collective-permute-start(bf16[1,1536,512]{2,1,0:T(8,128)(2,1)S(1)} %bitcast.46), channel_id=1, source_target_pairs={{0,8},{8,16},{16,24},{1,9},{9,17},{17,25},{2,10},{10,18},{18,26},{... | collective-permute-start | bytes 4718600 | tf_op jit(solution)/shard_map/ppermute | solution.py:190
  79.9 7.6 %copy-start.13 = (f32[4]{0:T(128)S(1)}, f32[4]{0:T(128)}, u32[]{:S(2)}) copy-start(f32[4]{0:T(128)} %param.20) | copy-start | bytes 52
  79.9 89.6 %all-to-all-start.4 = ((bf16[4,128,768]{1,2,0:T(8,128)(2,1)}), bf16[4,128,768]{1,2,0:T(8,128)(2,1)}, u32[]{:S(2)}, u32[]{:S(2)}) async-start(bf16[4,128,768]{1,2,0:T(8,128)(2,1)} %bitcast.63), calls=%async_computation.4 | async-start | bytes 1572864 | tf_op jit(solution)/shard_map/all_to_all | solution.py:214
  85.3 171.8 %all-gather.6.cloned.1.call-start = ((), (), s32[]{:S(2)}) async-start(), calls=%async_computation.6 | async-start | bytes 3932160 | tf_op jit(solution)/shard_map/all_gather | solution.py:215
  85.3 84.2 %collective-permute-start.1 = (s32[1536]{0:T(1024)S(1)}, s32[1536]{0:T(1024)S(1)}, u32[]{:S(2)}, u32[]{:S(2)}) collective-permute-start(s32[1536]{0:T(1024)S(1)} %reshape.71), channel_id=1, source_target_pairs={{0,8},{8,16},{16,24},{1,9},{9,17},{17,25},{2,10},{10,18},{18,26},{... | collective-permute-start | bytes 18440 | tf_op jit(solution)/shard_map/ppermute | solution.py:158
  87.2 84.6 %copy-start.1 = (f32[256]{0:T(256)S(1)}, f32[256]{0:T(256)}, u32[]{:S(2)}) copy-start(f32[256]{0:T(256)} %param.22) | copy-start | bytes 3076
  191.4 0.9 copy-start
  205.3 2.8 collective-permute-start.2
  205.3 2.9 copy-start.2
  205.3 3.1 copy-start.5
  208.0 2.9 copy-start.9
  209.6 1.4 collective-permute-start.3
  211.2 21.5 %collective-permute-start.12 = (bf16[384,1024]{1,0:T(8,128)(2,1)S(1)}, bf16[384,1024]{1,0:T(8,128)(2,1)}, u32[]{:S(2)}, u32[]{:S(2)}) collective-permute-start(bf16[384,1024]{1,0:T(8,128)(2,1)S(1)} %fusion.16), channel_id=1, source_target_pairs={{0,6},{2,4},{4,2},{6,0},{1,7},{3,5},{5,3},{7,1},{8,14},{10,12},{12... | collective-permute-start | bytes 2359304 | tf_op jit(solution)/shard_map/ppermute | solution.py:60
  212.7 35.0 %collective-permute-start.6 = (bf16[384,1024]{1,0:T(8,128)(2,1)S(1)}, bf16[384,1024]{1,0:T(8,128)(2,1)S(1)}, u32[]{:S(2)}, u32[]{:S(2)}) collective-permute-start(bf16[384,1024]{1,0:T(8,128)(2,1)S(1)} %fusion.16), channel_id=1, source_target_pairs={{0,2},{2,0},{4,6},{6,4},{1,3},{3,1},{5,7},{7,5},{8,10},{10,8},{12,... | collective-permute-start | bytes 2359304 | tf_op jit(solution)/shard_map/ppermute | solution.py:60
  213.1 35.7 %collective-permute-start.7 = (bf16[384,1024]{1,0:T(8,128)(2,1)S(1)}, bf16[384,1024]{1,0:T(8,128)(2,1)S(1)}, u32[]{:S(2)}, u32[]{:S(2)}) collective-permute-start(bf16[384,1024]{1,0:T(8,128)(2,1)S(1)} %fusion.16), channel_id=1, source_target_pairs={{0,4},{2,6},{4,0},{6,2},{1,5},{3,7},{5,1},{7,3},{8,12},{10,14},{12... | collective-permute-start | bytes 2359304 | tf_op jit(solution)/shard_map/ppermute | solution.py:60
  232.7 21.2 %collective-permute-start.13 = (bf16[384,1024]{1,0:T(8,128)(2,1)}, bf16[384,1024]{1,0:T(8,128)(2,1)}, u32[]{:S(2)}, u32[]{:S(2)}) collective-permute-start(bf16[384,1024]{1,0:T(8,128)(2,1)} %collective-permute-done.12), channel_id=1, source_target_pairs={{0,1},{1,0},{2,3},{3,2},{4,5},{5,4},{6,7},{7,6},{8,9},{9,8},{10,11... | collective-permute-start | bytes 2359304 | tf_op jit(solution)/shard_map/ppermute | solution.py:17
  249.7 9.9 %collective-permute-start.8 = (bf16[768,1024]{1,0:T(8,128)(2,1)}, bf16[768,1024]{1,0:T(8,128)(2,1)}, u32[]{:S(2)}, u32[]{:S(2)}) collective-permute-start(bf16[768,1024]{1,0:T(8,128)(2,1)} %constant_dynamic-update-slice_fusion), channel_id=1, source_target_pairs={{0,1},{1,0},{2,3},{3,2},{4,5},{5,4},{6,7},{7,6},{8,9},{9,8},{10,11... | collective-permute-start | bytes 4718600 | tf_op jit(solution)/shard_map/ppermute | solution.py:17
  249.8 24.2 %collective-permute-start.4 = (bf16[384,1024]{1,0:T(8,128)(2,1)S(1)}, bf16[384,1024]{1,0:T(8,128)(2,1)S(1)}, u32[]{:S(2)}, u32[]{:S(2)}) collective-permute-start(bf16[384,1024]{1,0:T(8,128)(2,1)S(1)} %fusion.16), channel_id=1, source_target_pairs={{0,1},{1,0},{2,3},{3,2},{4,5},{5,4},{6,7},{7,6},{8,9},{9,8},{10,11... | collective-permute-start | bytes 2359304 | tf_op jit(solution)/shard_map/ppermute | solution.py:17
  250.3 4.0 %copy-start.11 = (bf16[2048,1536]{1,0:T(8,128)(2,1)S(1)}, bf16[2048,1536]{1,0:T(8,128)(2,1)}, u32[]{:S(2)}) copy-start(bf16[2048,1536]{1,0:T(8,128)(2,1)} %all-gather.4.cloned.1.call-done) | copy-start | bytes 18874372
  257.1 7.6 %slice-start = ((s8[6291456]{0:T(1024)(128)(4,1)}), s8[4194304]{0:T(1024)(128)(4,1)S(1)}, s32[]{:S(2)}) async-start(s8[6291456]{0:T(1024)(128)(4,1)} %bitcast.66), calls=%async_computation.7 | async-start | bytes 8388608
  259.5 5.2 %slice-start.1 = ((s8[6291456]{0:T(1024)(128)(4,1)}), s8[2097152]{0:T(1024)(128)(4,1)S(1)}, s32[]{:S(2)}) async-start(s8[6291456]{0:T(1024)(128)(4,1)} %bitcast.66), calls=%async_computation.8 | async-start | bytes 4194304
  259.5 17.4 %collective-permute-start.14 = (bf16[384,1024]{1,0:T(8,128)(2,1)S(1)}, bf16[384,1024]{1,0:T(8,128)(2,1)S(1)}, u32[]{:S(2)}, u32[]{:S(2)}) collective-permute-start(bf16[384,1024]{1,0:T(8,128)(2,1)S(1)} %convolution_convert_fusion.1), channel_id=1, source_target_pairs={{0,1},{1,0},{2,3},{3,2},{4,5},{5,4},{6,7},{7,6},{8,9},{9,8},{10,11... | collective-permute-start | bytes 2359304 | tf_op jit(solution)/shard_map/ppermute | solution.py:17
  268.7 1.9 copy-start.12
  272.1 7.8 %collective-permute-start.9 = (bf16[768,1024]{1,0:T(8,128)(2,1)S(1)}, bf16[768,1024]{1,0:T(8,128)(2,1)S(1)}, u32[]{:S(2)}, u32[]{:S(2)}) collective-permute-start(bf16[768,1024]{1,0:T(8,128)(2,1)S(1)} %convolution_convert_fusion), channel_id=1, source_target_pairs={{0,1},{1,0},{2,3},{3,2},{4,5},{5,4},{6,7},{7,6},{8,9},{9,8},{10,11... | collective-permute-start | bytes 4718600 | tf_op jit(solution)/shard_map/ppermute | solution.py:17
  276.7 7.0 %collective-permute-start.5 = (bf16[384,1024]{1,0:T(8,128)(2,1)S(1)}, bf16[384,1024]{1,0:T(8,128)(2,1)S(1)}, u32[]{:S(2)}, u32[]{:S(2)}) collective-permute-start(bf16[384,1024]{1,0:T(8,128)(2,1)S(1)} %convolution_convert_fusion.2), channel_id=1, source_target_pairs={{0,1},{1,0},{2,3},{3,2},{4,5},{5,4},{6,7},{7,6},{8,9},{9,8},{10,11... | collective-permute-start | bytes 2359304 | tf_op jit(solution)/shard_map/ppermute | solution.py:17
  277.7 21.4 %collective-permute-start.15 = (bf16[384,1024]{1,0:T(8,128)(2,1)S(1)}, bf16[384,1024]{1,0:T(8,128)(2,1)S(1)}, u32[]{:S(2)}, u32[]{:S(2)}) collective-permute-start(bf16[384,1024]{1,0:T(8,128)(2,1)S(1)} %add_convert_fusion.1), channel_id=1, source_target_pairs={{0,6},{2,4},{4,2},{6,0},{1,7},{3,5},{5,3},{7,1},{8,14},{10,12},{12... | collective-permute-start | bytes 2359304 | tf_op jit(solution)/shard_map/ppermute | solution.py:60
  281.4 33.9 %collective-permute-start.11 = (bf16[384,1024]{1,0:T(8,128)(2,1)S(1)}, bf16[384,1024]{1,0:T(8,128)(2,1)S(1)}, u32[]{:S(2)}, u32[]{:S(2)}) collective-permute-start(bf16[384,1024]{1,0:T(8,128)(2,1)S(1)} %get-tuple-element.20), channel_id=1, source_target_pairs={{0,4},{2,6},{4,0},{6,2},{1,5},{3,7},{5,1},{7,3},{8,12},{10,14},{12... | collective-permute-start | bytes 2359304 | tf_op jit(solution)/shard_map/ppermute | solution.py:60
  282.4 33.1 %collective-permute-start.10 = (bf16[384,1024]{1,0:T(8,128)(2,1)S(1)}, bf16[384,1024]{1,0:T(8,128)(2,1)S(1)}, u32[]{:S(2)}, u32[]{:S(2)}) collective-permute-start(bf16[384,1024]{1,0:T(8,128)(2,1)S(1)} %get-tuple-element.19), channel_id=1, source_target_pairs={{0,2},{2,0},{4,6},{6,4},{1,3},{3,1},{5,7},{7,5},{8,10},{10,8},{12,... | collective-permute-start | bytes 2359304 | tf_op jit(solution)/shard_map/ppermute | solution.py:60
Sparse Core Ops, SparseCore 0:
  40.8 142.5 all-gather.3
  184.9 66.5 all-gather.5
